TPU v7x, 128 devices: a whole 4x4x4 slice. The times are simulated.
128 devices in a mesh: sp: 16 (over z, x), tp: 8 (over y, core).
Axes of the slice: x: 4, y: 4, z: 4, core: 2. Of those that a mesh axis runs over, the one named last changes fastest.
Arguments:
- tokens: bfloat16 [8192, 4096], P('sp'), may hold values from -6 to 6
- norm_gain: float32 [4096], replicated, may hold values from 0.1 to 1.9
- w_pool_in: bfloat16 [4096, 2048], P(None, 'tp'), may hold values from -0.09375 to 0.09375
- w_query: bfloat16 [4096, 2048], P(None, 'tp'), may hold values from -0.15625 to 0.15625
- w_key: bfloat16 [4096, 2048], P(None, 'tp'), may hold values from -0.15625 to 0.15625
- w_value: bfloat16 [4096, 2048], P(None, 'tp'), may hold values from -0.09375 to 0.09375
- pool_mix: bfloat16 [32, 64, 64], P('tp'), may hold values from -0.75 to 0.75
- pool_scale: float32 [2048], P('tp'), may hold values from 0.1 to 1.9
- lam: float32 [16], P('tp'), may hold values from 0.3 to 0.8
- head_gain: float32 [128], replicated, may hold values from 0.1 to 1.9
- pool_proj: bfloat16 [2048, 4096], P('tp'), may hold values from -0.125 to 0.125
- attn_proj: bfloat16 [2048, 4096], P('tp'), may hold values from -0.125 to 0.125
Outputs:
- mixed: bfloat16 [8192, 4096], P(('sp', 'tp'))
All inputs are finite; a program needn't handle non-finite values.
Results may differ from a plain program's by a relative error of at most 0.015.
Values may be sent and summed in bfloat16 or wider, within the bound.
A program may use at most 128 MiB of HBM per device.

v0:
```python
import jax
import jax.numpy as jnp
from jax import lax
from jax.sharding import PartitionSpec as P

GDIM = 64
HEAD = 64
VDIM = 128
SEGMENT = 64
REACH = 16


eps_norm = 1e-06
neg_big = -1e30
out_scale = 0.8


def passed_along(shard, axis, by):
    devices = lax.axis_size(axis)
    pairs = [(i, i + by) for i in range(devices) if 0 <= i + by < devices]
    return lax.ppermute(shard, axis, pairs)


def sent_together(arrays, axis, dim, along):
    widths = [a.shape[along] for a in arrays]
    both = jnp.concatenate(arrays, axis=along)
    whole = lax.all_gather(both, axis, axis=dim, tiled=True)
    return tuple(jnp.split(whole, [sum(widths[:k]) for k in range(1, len(widths))], axis=along))


def normalize(rows_in, gain):
    wide = rows_in.astype(jnp.float32)
    scaled = wide * lax.rsqrt(jnp.mean(wide * wide, axis=-1, keepdims=True) + eps_norm) * gain
    return scaled.astype(jnp.bfloat16)


def pooling(pool_in, rim, pool_mix, pool_scale, group_first, offset):
    count_rows, width = pool_in.shape
    padded = jnp.concatenate([rim, pool_in], 0).astype(jnp.float32)
    channel_group = group_first + jnp.arange(width, dtype=jnp.int32) // GDIM
    window = 2 ** (1 + channel_group % 4)
    total = jnp.zeros((count_rows, width), jnp.float32)
    for back in range(REACH):
        low = REACH - 1 - back
        total = total + jnp.where(back < window[None, :], padded[low : low + count_rows], 0.0)
    position = offset + jnp.arange(count_rows, dtype=jnp.int32)
    count = jnp.minimum(position[:, None] + 1, window[None, :]).astype(jnp.float32)
    pooled = (total / count - pool_in.astype(jnp.float32)).astype(jnp.bfloat16)
    groups = pool_mix.shape[0]
    grouped = jnp.einsum(
        "sgi,gio->sgo",
        pooled.reshape(count_rows, groups, GDIM),
        pool_mix,
        preferred_element_type=jnp.float32,
    )
    return (grouped.reshape(count_rows, width) * pool_scale).astype(jnp.bfloat16)


def attend_block(carry, query, keys, values, key_start, query_start):
    peak, weight_sum, weighted = carry
    key_seg = (key_start + jnp.arange(keys.shape[0], dtype=jnp.int32)) // SEGMENT
    query_seg = (query_start + jnp.arange(query.shape[0], dtype=jnp.int32)) // SEGMENT
    allowed = key_seg[None, :] <= query_seg[:, None]
    scores = jnp.einsum(
        "qhmd,khmd->hmqk", query, keys, preferred_element_type=jnp.float32
    ) * HEAD ** (-0.5)
    masked = jnp.where(allowed, scores, neg_big)
    new_peak = jnp.maximum(peak, jnp.max(masked, axis=-1))
    probs = jnp.where(allowed, jnp.exp(masked - new_peak[..., None]), 0.0)
    shrink = jnp.exp(peak - new_peak)
    weight_sum = weight_sum * shrink + jnp.sum(probs, axis=-1)
    weighted = weighted * shrink[..., None] + jnp.einsum(
        "hmqk,khe->hmqe", probs.astype(jnp.bfloat16), values, preferred_element_type=jnp.float32
    )
    return (new_peak, weight_sum, weighted)


def guarded(carry, key_start, key_count, query, query_start, make_keys):
    heads = query.shape[1]
    last_seg = (query_start + query.shape[0] - 1) // SEGMENT

    def update(carry_now):
        keys, values = make_keys()
        keys = keys.reshape(key_count, heads, 2, HEAD)
        values = values.reshape(key_count, heads, VDIM)
        return attend_block(carry_now, query, keys, values, key_start, query_start)

    return lax.cond(key_start // SEGMENT > last_seg, lambda carry_now: carry_now, update, carry)


def sweep(carry, piece, step_fn):
    count_rows = jax.tree.leaves(piece)[0].shape[0]
    block = 512

    def one(carry_now, index):
        first = index * block
        part = jax.tree.map(lambda array: lax.dynamic_slice_in_dim(array, first, block, 0), piece)
        return (step_fn(carry_now, part, first, block), None)

    carry, unused = lax.scan(one, carry, jnp.arange(count_rows // block, dtype=jnp.int32))
    return carry


def body(
    tokens,
    norm_gain,
    w_pool_in,
    w_query,
    w_key,
    w_value,
    pool_mix,
    pool_scale,
    lam,
    head_gain,
    pool_proj,
    attn_proj,
):
    count_rows = tokens.shape[0]
    offset = lax.axis_index("sp") * count_rows
    normed = normalize(tokens, norm_gain)
    pool_in = jnp.dot(normed, w_pool_in, preferred_element_type=jnp.float32).astype(jnp.bfloat16)
    query = jnp.dot(normed, w_query, preferred_element_type=jnp.float32).astype(jnp.bfloat16)
    heads = w_value.shape[1] // VDIM
    query_heads = query.reshape(count_rows, heads, 2, HEAD)
    rim = passed_along(pool_in[count_rows - (REACH - 1) :], "sp", 1)
    group_first = lax.axis_index("tp") * pool_mix.shape[0]
    pool_out = pooling(pool_in, rim, pool_mix, pool_scale, group_first, offset)
    start_carry = (
        jnp.full((heads, 2, count_rows), neg_big, jnp.float32),
        jnp.zeros((heads, 2, count_rows), jnp.float32),
        jnp.zeros((heads, 2, count_rows, VDIM), jnp.float32),
    )
    keys = jnp.dot(normed, w_key, preferred_element_type=jnp.float32).astype(jnp.bfloat16)
    values = jnp.dot(normed, w_value, preferred_element_type=jnp.float32).astype(jnp.bfloat16)

    def add_keys(carry, piece):

        def step(carry_now, part, part_start, block):
            return guarded(
                carry_now, part_start, block, query_heads, offset, lambda: (part[0], part[1])
            )

        return sweep(carry, piece, step)

    carry = add_keys(start_carry, sent_together((keys, values), "sp", 0, 1))
    peak, weight_sum, weighted = carry
    averaged = weighted / weight_sum[..., None]
    blend = averaged[:, 0] - lam[:, None, None] * averaged[:, 1]
    scaled = (
        blend
        * lax.rsqrt(jnp.mean(blend * blend, axis=-1, keepdims=True) + eps_norm)
        * head_gain
        * out_scale
    )
    attn_out = scaled.astype(jnp.bfloat16).transpose(1, 0, 2).reshape(count_rows, heads * VDIM)
    term = jnp.dot(pool_out, pool_proj, preferred_element_type=jnp.float32)
    return lax.psum_scatter(
        (term + jnp.dot(attn_out, attn_proj, preferred_element_type=jnp.float32)).astype(
            jnp.bfloat16
        ),
        "tp",
        scatter_dimension=0,
        tiled=True,
    )


def solution(mesh):
    return jax.shard_map(
        body,
        mesh=mesh,
        in_specs=(
            P("sp", None),
            P(),
            P(None, "tp"),
            P(None, "tp"),
            P(None, "tp"),
            P(None, "tp"),
            P("tp", None, None),
            P("tp"),
            P("tp"),
            P(),
            P("tp", None),
            P("tp", None),
        ),
        out_specs=P(("sp", "tp"), None),
        check_vma=False,
    )
```

profile of v0, /device:TPU:32, one launch (start us, length us, event | category | flops | bytes accessed | tf_op | source)
XLA Modules:
  0.0 264.6 jit_solution(14030497630168138699)
XLA Ops:
  6.5 3.2 %fusion.18 = f32[512]{0:T(512)S(1)} fusion(bf16[512,4096]{1,0:T(8,128)(2,1)} %param.16), kind=kLoop, calls=%fused_computation.36 | loop fusion | flops 6290944 | bytes 4196352 | tf_op jit(solution)/shard_map/reduce_sum | solution.py:33
  10.1 2.5 fusion.20
  12.7 1.3 convolution_convert_fusion.1
  15.8 1.3 convolution_convert_fusion.2
  18.0 4.1 %convolution_convert_fusion.3 = bf16[512,256]{1,0:T(8,128)(2,1)S(1)} fusion(bf16[512,4096]{1,0:T(8,128)(2,1)} %copy-done.2, bf16[4096,256]{1,0:T(8,128)(2,1)} %param.18), kind=kOutput, calls=%fused_computation.43 | convolution fusion | flops 1073872896 | bytes 6553600 | tf_op jit(solution)/shard_map/dot_general | solution.py:121
  22.2 3.6 %collective-permute-start = (bf16[15,256]{1,0:T(8,128)(2,1)S(1)}, bf16[15,256]{1,0:T(8,128)(2,1)S(1)}, u32[]{:S(2)}, u32[]{:S(2)}) collective-permute-start(bf16[15,256]{1,0:T(8,128)(2,1)S(1)} %slice.76), channel_id=1, source_target_pairs={{0,8},{8,16},{16,24},{24,32},{32,40},{40,48},{48,56},{56,64},{64,7... | collective-permute-start | bytes 23048 | tf_op jit(solution)/shard_map/ppermute | solution.py:21
  26.0 4.2 %convolution_convert_fusion = bf16[512,256]{0,1:T(8,128)(2,1)S(1)} fusion(bf16[512,4096]{1,0:T(8,128)(2,1)} %copy-done.2, bf16[4096,256]{1,0:T(8,128)(2,1)} %param.19), kind=kOutput, calls=%fused_computation.40 | convolution fusion | flops 1073872896 | bytes 6553600 | tf_op jit(solution)/shard_map/dot_general | solution.py:122
  30.3 1.2 fusion.41
  32.0 4.5 %fusion.47 = f32[512,4096]{1,0:T(8,128)} fusion(bf16[512,256]{0,1:T(8,128)(2,1)S(1)} %fusion.40, bf16[256,4096]{1,0:T(8,128)(2,1)S(1)} %copy-done), kind=kOutput, calls=%fused_computation.126 | convolution fusion | flops 1073741824 | bytes 10747904 | tf_op jit(solution)/shard_map/dot_general | solution.py:156
  36.5 60.6 %all-gather.2.cloned.1.call-done = bf16[8192,512]{0,1:T(8,128)(2,1)} async-done(((bf16[512,512]{0,1:T(8,128)(2,1)}), bf16[8192,512]{0,1:T(8,128)(2,1)}) %all-gather.2.cloned.1.call-update) | async-done | bytes 8388624 | tf_op jit(solution)/shard_map/all_gather | solution.py:27
  97.1 5.9 %fusion.45 = (bf16[8192,256]{0,1:T(8,128)(2,1)}, bf16[8192,256]{0,1:T(8,128)(2,1)}) fusion(bf16[8192,512]{0,1:T(8,128)(2,1)} %all-gather.2.cloned.1.call-done), kind=kLoop, calls=%fused_computation.124 | loop fusion | bytes 16777216 | tf_op jit(solution)/shard_map/split | solution.py:28
  103.1 48.3 %while.17 = (s32[]{:T(128)}, f32[2,2,512]{2,1,0:T(2,128)S(1)}, f32[2,2,512]{2,1,0:T(2,128)S(1)}, f32[2,2,512,128]{3,2,1,0:T(8,128)S(1)}, s32[16]{0:T(128)S(1)}, ...) while((s32[]{:T(128)}, f32[2,2,512]{2,1,0:T(2,128)S(1)}, ...), condition=%wide.region_6.7_spmd, body=%wide.region_1.6_spmd.sunk | while | flops 417091616 | bytes 17703412 | solution.py:100
  104.4 5.4 %conditional.2 = (f32[2,2,512]{2,1,0:T(2,128)S(1)}, f32[2,2,512]{2,1,0:T(2,128)S(1)}, f32[2,2,512,128]{3,2,1,0:T(8,128)S(1)}) conditional(s32[]{:T(128)} %convert_element_type.94, (s32[]{:T(128)}, s32[]{:T(128)}, pred[]{:T(512)}, bf16[8192,256]{0,1:T(8,128)(2,1)}, bf16[512,2,2,64]{0,3,2,1:T(8,128)(2,1)S(1)}, /*index=5*/f32[2,2,512]{2,1,0:T(2,128)S(1)}, ...), branch_computations={%region_2.4_spmd, %region_5.5_spmd} | conditional | flops 417091584 | bytes 17686588 | solution.py:88
  104.4 1.3 constant_dynamic-slice_fusion
  107.0 1.0 fusion.2
  108.0 1.8 fusion.6
  111.1 5.4 %conditional.2 = (f32[2,2,512]{2,1,0:T(2,128)S(1)}, f32[2,2,512]{2,1,0:T(2,128)S(1)}, f32[2,2,512,128]{3,2,1,0:T(8,128)S(1)}) conditional(s32[]{:T(128)} %convert_element_type.94, (s32[]{:T(128)}, s32[]{:T(128)}, pred[]{:T(512)}, bf16[8192,256]{0,1:T(8,128)(2,1)}, bf16[512,2,2,64]{0,3,2,1:T(8,128)(2,1)S(1)}, /*index=5*/f32[2,2,512]{2,1,0:T(2,128)S(1)}, ...), branch_computations={%region_2.4_spmd, %region_5.5_spmd} | conditional | flops 417091584 | bytes 17686588 | solution.py:88
  111.2 1.3 constant_dynamic-slice_fusion
  114.8 1.8 fusion.6
  117.9 5.4 %conditional.2 = (f32[2,2,512]{2,1,0:T(2,128)S(1)}, f32[2,2,512]{2,1,0:T(2,128)S(1)}, f32[2,2,512,128]{3,2,1,0:T(8,128)S(1)}) conditional(s32[]{:T(128)} %convert_element_type.94, (s32[]{:T(128)}, s32[]{:T(128)}, pred[]{:T(512)}, bf16[8192,256]{0,1:T(8,128)(2,1)}, bf16[512,2,2,64]{0,3,2,1:T(8,128)(2,1)S(1)}, /*index=5*/f32[2,2,512]{2,1,0:T(2,128)S(1)}, ...), branch_computations={%region_2.4_spmd, %region_5.5_spmd} | conditional | flops 417091584 | bytes 17686588 | solution.py:88
  117.9 1.3 constant_dynamic-slice_fusion
  121.5 1.8 fusion.6
  124.6 5.4 %conditional.2 = (f32[2,2,512]{2,1,0:T(2,128)S(1)}, f32[2,2,512]{2,1,0:T(2,128)S(1)}, f32[2,2,512,128]{3,2,1,0:T(8,128)S(1)}) conditional(s32[]{:T(128)} %convert_element_type.94, (s32[]{:T(128)}, s32[]{:T(128)}, pred[]{:T(512)}, bf16[8192,256]{0,1:T(8,128)(2,1)}, bf16[512,2,2,64]{0,3,2,1:T(8,128)(2,1)S(1)}, /*index=5*/f32[2,2,512]{2,1,0:T(2,128)S(1)}, ...), branch_computations={%region_2.4_spmd, %region_5.5_spmd} | conditional | flops 417091584 | bytes 17686588 | solution.py:88
  124.6 1.3 constant_dynamic-slice_fusion
  128.2 1.8 fusion.6
  131.3 5.4 %conditional.2 = (f32[2,2,512]{2,1,0:T(2,128)S(1)}, f32[2,2,512]{2,1,0:T(2,128)S(1)}, f32[2,2,512,128]{3,2,1,0:T(8,128)S(1)}) conditional(s32[]{:T(128)} %convert_element_type.94, (s32[]{:T(128)}, s32[]{:T(128)}, pred[]{:T(512)}, bf16[8192,256]{0,1:T(8,128)(2,1)}, bf16[512,2,2,64]{0,3,2,1:T(8,128)(2,1)S(1)}, /*index=5*/f32[2,2,512]{2,1,0:T(2,128)S(1)}, ...), branch_computations={%region_2.4_spmd, %region_5.5_spmd} | conditional | flops 417091584 | bytes 17686588 | solution.py:88
  131.4 1.3 constant_dynamic-slice_fusion
  135.0 1.8 fusion.6
  151.5 1.4 copy.23
  152.9 1.5 broadcast_divide_fusion
  154.8 6.7 %add_convert_fusion = bf16[512,4096]{1,0:T(8,128)(2,1)} fusion(f32[512,4096]{1,0:T(8,128)} %fusion.47, bf16[512,256]{0,1:T(8,128)(2,1)S(1)} %bitcast.70, bf16[256,4096]{1,0:T(8,128)(2,1)S(1)} %copy-done.3), kind=kOutput, calls=%fused_computation.39 | convolution fusion | flops 1077936128 | bytes 14942208 | tf_op jit(solution)/shard_map/dot_general | solution.py:158
  161.5 96.2 %reduce-scatter.2.cloned.1.call-done = bf16[64,4096]{1,0:T(8,128)(2,1)} async-done(((bf16[512,4096]{1,0:T(8,128)(2,1)}), bf16[64,4096]{1,0:T(8,128)(2,1)}) %reduce-scatter.2.cloned.1.call-update) | async-done | bytes 524304 | tf_op jit(solution)/shard_map/reduce_scatter | solution.py:157
  (133 shorter events, 24.2 us)
Async XLA Ops:
  6.5 25.5 %copy-start = (bf16[256,4096]{1,0:T(8,128)(2,1)S(1)}, bf16[256,4096]{1,0:T(8,128)(2,1)}, u32[]{:S(2)}) copy-start(bf16[256,4096]{1,0:T(8,128)(2,1)} %param.26) | copy-start | bytes 6291460
  6.5 90.6 %all-gather.2.cloned.1.call-start = ((), (), s32[]{:S(2)}) async-start(), calls=%async_computation.1 | async-start | bytes 8912896 | tf_op jit(solution)/shard_map/all_gather | solution.py:27
  6.5 3.6 %copy-start.1 = (bf16[512,4096]{1,0:T(8,128)(2,1)S(1)}, bf16[512,4096]{1,0:T(8,128)(2,1)}, u32[]{:S(2)}) copy-start(bf16[512,4096]{1,0:T(8,128)(2,1)} %param.16) | copy-start | bytes 12582916
  10.1 2.5 copy-start.8
  12.7 2.1 copy-start.2
  12.7 3.1 %copy-start.9 = (bf16[4096,256]{1,0:T(8,128)(2,1)S(1)}, bf16[4096,256]{1,0:T(8,128)(2,1)}, u32[]{:S(2)}) copy-start(bf16[4096,256]{1,0:T(8,128)(2,1)} %param.20) | copy-start | bytes 6291460
  18.0 239.7 %reduce-scatter.2.cloned.1.call-start = ((), (), s32[]{:S(2)}) async-start(), calls=%async_computation.2 | async-start | bytes 4718592 | tf_op jit(solution)/shard_map/reduce_scatter | solution.py:157
  22.2 8.0 %collective-permute-start = (bf16[15,256]{1,0:T(8,128)(2,1)S(1)}, bf16[15,256]{1,0:T(8,128)(2,1)S(1)}, u32[]{:S(2)}, u32[]{:S(2)}) collective-permute-start(bf16[15,256]{1,0:T(8,128)(2,1)S(1)} %slice.76), channel_id=1, source_target_pairs={{0,8},{8,16},{16,24},{24,32},{32,40},{40,48},{48,56},{56,64},{64,7... | collective-permute-start | bytes 23048 | tf_op jit(solution)/shard_map/ppermute | solution.py:21
  30.3 1.3 copy-start.4
  30.3 1.6 copy-start.6
  151.4 3.0 %copy-start.5 = (f32[2]{0:T(128)S(1)}, f32[2]{0:T(128)}, u32[]{:S(2)}) copy-start(f32[2]{0:T(128)} %param.24) | copy-start | bytes 28
  151.4 3.2 %copy-start.7 = (f32[128]{0:T(128)S(1)}, f32[128]{0:T(128)}, u32[]{:S(2)}) copy-start(f32[128]{0:T(128)} %param.25) | copy-start | bytes 1540
  152.9 1.9 copy-start.3
Sparse Core Ops, SparseCore 0:
  18.1 78.9 all-gather.1
  161.7 96.0 reduce-scatter.1
where the time goes:
time: 266 us; the launch traced here: 265 us
  waiting for transfers between devices  157 us (59%)
  matrix products  36.1 us (14%)
  local copies, waits for them, and re-layouts  25.9 us (10%)
  other arithmetic  16.5 us (6%)
  between operations  13.7 us (5%)
  loops' own time  12 us (5%)
  starting transfers between devices  3.62 us (1%)
    reduce_scatter x1, waiting for transfers between devices, body(): lax.psum_scatter((term + jnp.dot(attn_out, attn_proj, preferred_element_t...  96.2 us
    all_gather x1, waiting for transfers between devices, sent_together(): whole = lax.all_gather(both, axis, axis=dim, tiled=True)  60.6 us
    another operation x1, loops' own time, sweep(): lax.scan(one, carry, jnp.arange(count_rows // block, dtype=jnp.int32))  11.4 us
    dynamic_slice x16, local copies, waits for them, and re-layouts, sweep(): lax.scan(one, carry, jnp.arange(count_rows // block, dtype=jnp.int32))  9.38 us
    dot_general x5, matrix products, attend_block(): jnp.einsum('hmqk,khe->hmqe', probs.astype(jnp.bfloat16), values, preferre...  9.04 us
    dynamic_slice x5, local copies, waits for them, and re-layouts, one(): lax.dynamic_slice_in_dim(array, first, block, 0)  6.72 us
    dot_general x1, matrix products, body(): jnp.dot(attn_out, attn_proj, preferred_element_type=jnp.float32)  6.72 us
    split x1, local copies, waits for them, and re-layouts, sent_together(): jnp.split(whole, [sum(widths[:k]) for k in range(1, len(widths))], axis=a...  5.9 us
  transfers between devices with their start and end apart: 3, of which 2 were waited for; matrix products, arithmetic and copies ran while one was open for 6% of the time, Pallas kernels for 0%

commit v1 on v0

v1 whole, which is shorter than its diff:
```python
import jax
import jax.numpy as jnp
from jax import lax
from jax.experimental import pallas as pl
from jax.experimental.pallas import tpu as pltpu
from jax.sharding import PartitionSpec as P

EPS = 1e-6
NEG = -1e30
LOG2E = 1.4426950408889634
ROWS = 512
WIDE = 4096
SEG = 64
BF = jnp.bfloat16
F32 = jnp.float32
MESH_ID = pl.DeviceIdType.MESH
ANY = pl.BlockSpec(memory_space=pl.ANY)
VM = pl.BlockSpec(memory_space=pltpu.VMEM)
SM = pl.BlockSpec(memory_space=pltpu.SMEM)


def project_kernel(tok, gain, w_k, w_v, w_q, w_p, lam, kv_out, q_out, pool_out, lam_out,
                   raw, normed, wts, tok_sem, w_sem):
    loads = []
    for r in range(4):
        cp = pltpu.make_async_copy(tok.at[pl.ds(r * 128, 128)], raw.at[pl.ds(r * 128, 128)], tok_sem.at[r])
        cp.start()
        loads.append(cp)
    w_loads = []
    for i, w in enumerate((w_k, w_v, w_q, w_p)):
        cp = pltpu.make_async_copy(w, wts.at[i], w_sem.at[i])
        cp.start()
        w_loads.append(cp)
    for hh in range(2):
        lam_out[hh] = jnp.full((8, 128), lam[hh], F32)

    for r in range(4):
        loads[r].wait()

        @pl.loop(0, 8)
        def _(i):
            rows = pl.ds(pl.multiple_of(r * 128 + i * 16, 16), 16)
            wide = raw[rows].astype(F32)
            scale = lax.rsqrt(jnp.mean(wide * wide, axis=-1, keepdims=True) + EPS)
            normed[rows] = (wide * scale * gain[...]).astype(BF)

    def product(i):
        w_loads[i].wait()
        return jnp.dot(normed[...], wts[i], preferred_element_type=F32)

    keys = product(0).astype(BF)
    for hh in range(2):
        for hf in range(2):
            kv_out[hh, hf, 0:256] = keys[256 * hf:256 * hf + 256, 128 * hh:128 * hh + 128]
    values = product(1)
    for hh in range(2):
        for hf in range(2):
            for j in range(2):
                first = 256 * hf + 128 * j
                tile = values[first:first + 128, 128 * hh:128 * hh + 128]
                kv_out[hh, hf, 256 + 128 * j:384 + 128 * j] = tile.T.astype(BF)
    query = product(2).astype(BF)
    for hh in range(2):
        q_out[hh] = query[:, 128 * hh:128 * hh + 128]
    pool_out[...] = product(3).astype(BF)


def mixer_kernel(kv_in, q_in, pool_in, lam_in, pool_mix, pool_scale, head_gain, pool_proj, attn_proj,
                 out,
                 kv, qraw, qcat, lamb, rim, acc, top, den, ao, ab, pooled, w_out, pbuf, dbuf, sbuf, relay, fin,
                 w_sem, a2a_send, kv_recv, q_send, q_recv, lam_send, lam_recv, rim_send, rim_recv,
                 zp_send, zm_send, dd_send, ret_send, ret_recv, pd_send, pd_recv, y_send, y_recv):
    sp = lax.axis_index("sp")
    tp = lax.axis_index("tp")
    z, x = lax.div(sp, 4), lax.rem(sp, 4)
    y, c = lax.div(tp, 2), lax.rem(tp, 2)

    def wrap(i):
        return lax.rem(i + 4, 4)

    def dev(zz, xx, cc):
        return (zz * 4 + xx, y * 2 + cc)

    me = (sp, tp)

    def is_me(d):
        return (d[0] == sp) & (d[1] == tp)

    core_src = lax.div(x, 2)
    odd_row = lax.rem(z, 2) == 1
    zq = jnp.where(odd_row, 3 - x, x)
    cq = jnp.where((z == 0) | (z == 3), 0, 1)
    sq = lax.div(z, 2)
    qb = [jnp.where(c == 0, z, 7 - z), jnp.where(c == 0, 15 - z, 8 + z)]
    partner = dev(z, x, 1 - c)
    z_up, z_dn = dev(wrap(z + 1), x, c), dev(wrap(z - 1), x, c)
    y_up = (sp, wrap(y + 1) * 2 + c)
    y_dn = (sp, wrap(y - 1) * 2 + c)
    nxt = (lax.rem(sp + 1, 16), tp)
    prv = (lax.rem(sp + 15, 16), tp)
    a2a_dst = [[dev(z, 2 * c + hh, hf) for hf in range(2)] for hh in range(2)]
    q_dst = [dev(zq, 2 * c + hh, cq) for hh in range(2)]
    q_src = [dev(lax.div(qb[s], 4), lax.rem(qb[s], 4), core_src) for s in range(2)]

    w_loads = [pltpu.make_async_copy(pool_proj, w_out.at[pl.ds(0, 256)], w_sem.at[0]),
               pltpu.make_async_copy(attn_proj, w_out.at[pl.ds(256, 256)], w_sem.at[1])]
    for cp in w_loads:
        cp.start()

    barrier = pltpu.get_barrier_semaphore()

    def greet(d):
        pl.semaphore_signal(barrier, inc=1, device_id=d, device_id_type=MESH_ID)

    greeted = [dev(z, xk, core_src) for xk in range(4)] + q_src + q_dst + [z_up, z_dn, partner, y_up, y_dn, prv]
    for d in greeted:
        greet(d)
    pl.semaphore_wait(barrier, len(greeted))

    def remote(src, dst, ssem, rsem, d):
        return pltpu.make_async_remote_copy(src_ref=src, dst_ref=dst, send_sem=ssem, recv_sem=rsem,
                                            device_id=d, device_id_type=MESH_ID)

    def send_any(src, dst, ssem, rsem, d):
        @pl.when(is_me(d))
        def _():
            pltpu.make_async_copy(src, dst, rsem).start()

        @pl.when(jnp.logical_not(is_me(d)))
        def _():
            remote(src, dst, ssem, rsem, d).start()

    def sent_any(src, dst, ssem, rsem, d):
        @pl.when(jnp.logical_not(is_me(d)))
        def _():
            remote(src, dst, ssem, rsem, d).wait_send()

    def arrived(dst, rsem):
        pltpu.make_async_copy(dst, dst, rsem).wait()

    rim_args = (pool_in.at[pl.ds(ROWS - 16, 16)], rim, rim_send, rim_recv, nxt)
    remote(*rim_args).start()
    a2a_args = []
    for hh in range(2):
        for hf in range(2):
            a2a_args.append((kv_in.at[hh, hf], kv.at[z, hf, x], a2a_send.at[hh, hf], kv_recv.at[0, hf, x],
                             a2a_dst[hh][hf]))
    q_args = []
    for hh in range(2):
        q_args.append((q_in.at[hh], qraw.at[sq], q_send.at[hh], q_recv.at[sq], q_dst[hh]))
        q_args.append((lam_in.at[hh], lamb.at[sq], lam_send.at[hh], lam_recv.at[sq], q_dst[hh]))
    for a in a2a_args + q_args:
        send_any(*a)

    arrived(rim, rim_recv)
    remote(*rim_args).wait_send()
    edge = jnp.where(sp == 0, 0.0, rim[...].astype(F32))
    own = pool_in[...].astype(F32)
    line = jnp.concatenate([edge, own], axis=0)
    s2 = line + pltpu.roll(line, 1, 0)
    s4 = s2 + pltpu.roll(s2, 2, 0)
    s8 = s4 + pltpu.roll(s4, 4, 0)
    s16 = s8 + pltpu.roll(s8, 8, 0)
    lane = lax.broadcasted_iota(jnp.int32, (1, 256), 1)
    total = jnp.where(lane < 64, s2, jnp.where(lane < 128, s4, jnp.where(lane < 192, s8, s16)))[16:]
    window = jnp.where(lane < 64, 2, jnp.where(lane < 128, 4, jnp.where(lane < 192, 8, 16)))
    position = sp * ROWS + lax.broadcasted_iota(jnp.int32, (ROWS, 256), 0)
    count = jnp.minimum(position + 1, window).astype(F32)
    mixed_in = (total / count - own).astype(BF)
    spread = (lax.rem(lax.broadcasted_iota(jnp.int32, (64, 256), 1), 64)
              == lax.broadcasted_iota(jnp.int32, (64, 256), 0)).astype(F32).astype(BF)
    wide_mix = jnp.dot(pool_mix[...], spread, preferred_element_type=F32)
    same = (lax.div(lax.broadcasted_iota(jnp.int32, (256, 256), 0), 64)
            == lax.div(lax.broadcasted_iota(jnp.int32, (256, 256), 1), 64))
    block_mix = jnp.where(same, wide_mix, 0.0).astype(BF)
    grouped = jnp.dot(mixed_in, block_mix, preferred_element_type=F32)
    pooled[...] = (grouped * pool_scale[...]).astype(BF)

    def dd_args(rel, xk):
        piece = kv.at[wrap(z + rel), c, xk]
        return (piece, piece, dd_send.at[rel, xk], kv_recv.at[rel, c, xk], partner)

    def up_args(rel, xk):
        piece = kv.at[wrap(z + rel), c, xk]
        return (piece, piece, zp_send.at[rel & 1, xk], kv_recv.at[(rel + 3) % 4, c, xk], z_up)

    def dn_args(rel, xk):
        piece = kv.at[wrap(z + rel), c, xk]
        return (piece, piece, zm_send.at[rel & 1, xk], kv_recv.at[(rel + 1) % 4, c, xk], z_dn)

    def mine(rel, xk):
        arrived(kv.at[wrap(z + rel), c, xk], kv_recv.at[rel, c, xk])

    for xk in range(4):
        mine(0, xk)
        remote(*up_args(0, xk)).start()
        if xk >= 2:
            remote(*dn_args(0, xk)).start()
        remote(*dd_args(0, xk)).start()
    for xk in range(2):
        remote(*dn_args(0, xk)).start()

    for s in range(2):
        arrived(qraw.at[s], q_recv.at[s])
        arrived(lamb.at[s], lam_recv.at[s])
        q = qraw[s] * jnp.asarray(0.125, BF)
        first = lax.broadcasted_iota(jnp.int32, (ROWS, 128), 1) < 64
        qcat[s, 0] = jnp.where(first, q, jnp.zeros_like(q))
        qcat[s, 1] = jnp.where(first, jnp.zeros_like(q), q)
        for m in range(2):
            top[s, m] = jnp.full((1, ROWS), NEG, F32)
            den[s, m] = jnp.zeros((1, ROWS), F32)
            acc[s, m] = jnp.zeros((128, ROWS), F32)

    def attend(s, zk, xk, masked):
        halves = [kv[zk, hf, xk] for hf in range(2)]
        keys = jnp.concatenate([h[:256] for h in halves], axis=0)
        vals = jnp.concatenate([h[256 + 128 * j:384 + 128 * j] for h in halves for j in range(2)], axis=1)
        for m in range(2):
            scores = lax.dot_general(keys, qcat[s, m], (((1,), (1,)), ((), ())),
                                     preferred_element_type=F32) * LOG2E
            if masked:
                allowed = (lax.div(lax.broadcasted_iota(jnp.int32, (ROWS, ROWS), 0), SEG)
                           <= lax.div(lax.broadcasted_iota(jnp.int32, (ROWS, ROWS), 1), SEG))
                scores = jnp.where(allowed, scores, NEG)
            old = top[s, m]
            new = jnp.maximum(old, jnp.max(scores, axis=0, keepdims=True))
            probs = jnp.exp2(scores - new)
            shrink = jnp.exp2(old - new)
            top[s, m] = new
            den[s, m] = den[s, m] * shrink + jnp.sum(probs, axis=0, keepdims=True)
            acc[s, m] = acc[s, m] * shrink + jnp.dot(vals, probs.astype(BF), preferred_element_type=F32)

    def visit(rel, xk):
        zk = wrap(z + rel)
        arrived(kv.at[zk, 1 - c, xk], kv_recv.at[rel, 1 - c, xk])
        block = zk * 4 + xk

        @pl.loop(0, 2)
        def _(s):
            target = jnp.where(s == 0, qb[0], qb[1])

            @pl.when(block < target)
            def _():
                attend(s, zk, xk, False)

            @pl.when(block == target)
            def _():
                attend(s, zk, xk, True)

    @pl.loop(0, 4)
    def _(xk):
        visit(0, xk)

    @pl.loop(0, 5)
    def _(i):
        @pl.when(i < 4)
        def _():
            mine(3, i)
            remote(*dd_args(3, i)).start()

            @pl.when(i < 2)
            def _():
                remote(*up_args(3, i)).start()

            j = lax.rem(i + 2, 4)
            mine(1, j)
            remote(*dd_args(1, j)).start()

            @pl.when(i < 2)
            def _():
                remote(*dn_args(1, j)).start()

        @pl.when(i > 0)
        def _():
            @pl.loop(0, 2)
            def _(side):
                k = jnp.where(side == 0, i - 1, lax.rem(i + 1, 4))
                visit(jnp.where(side == 0, 3, 1), k)

    def turn(i):
        return jnp.where(i == 0, 0, jnp.where(i == 1, 2, jnp.where(i == 2, 1, 3)))

    @pl.loop(0, 5)
    def _(i):
        @pl.when(i < 4)
        def _():
            k = turn(i)
            mine(2, k)
            remote(*dd_args(2, k)).start()

        @pl.when(i > 0)
        def _():
            visit(2, turn(i - 1))

    ret_args = []
    for s in range(2):
        o1 = acc[s, 0] / den[s, 0]
        o2 = acc[s, 1] / den[s, 1]
        blend = o1 - lamb[s][0:1, 0:1] * o2
        scaled = blend * lax.rsqrt(jnp.mean(blend * blend, axis=0, keepdims=True) + EPS)
        ao[s] = (scaled.T * head_gain[...] * 0.8).astype(BF)
        mine_h = lax.rem(x, 2)
        a = (ao.at[s], ab.at[mine_h], ret_send.at[s], ret_recv.at[mine_h], q_src[s])
        send_any(*a)
        ret_args.append(a)

    for a in a2a_args + q_args:
        sent_any(*a)
    for xk in range(4):
        remote(*up_args(0, xk)).wait_send()
        remote(*dn_args(0, xk)).wait_send()
        for rel in range(4):
            remote(*dd_args(rel, xk)).wait_send()
    for xk in range(2):
        remote(*up_args(3, xk)).wait_send()
        remote(*dn_args(1, xk + 2)).wait_send()

    for cp in w_loads:
        cp.wait()
    for hh in range(2):
        arrived(ab.at[hh], ret_recv.at[hh])

    order = [wrap(y + 2), wrap(y + 1), wrap(y - 1), y]

    def pd_args(h, k):
        return (pbuf.at[h, 2 * order[k] + 1 - c], dbuf.at[h, k], pd_send.at[h, k], pd_recv.at[h, k], partner)

    for h in range(2):
        @pl.loop(0, 4)
        def _(n):
            cols = pl.ds(pl.multiple_of(h * 2048 + n * 512, 512), 512)
            to = pl.ds(pl.multiple_of(n * 512, 512), 512)
            feats = jnp.concatenate([pooled[...], ab[0], ab[1]], axis=1)
            term = jnp.dot(feats, w_out[:, cols], preferred_element_type=F32)
            pbuf[h, :, :, to] = term.astype(BF).reshape(8, 64, 512)

        for k in range(4):
            remote(*pd_args(h, k)).start()

    def chip_sum(h, k):
        arrived(dbuf.at[h, k], pd_recv.at[h, k])
        return pbuf[h, 2 * order[k] + c].astype(F32) + dbuf[h, k].astype(F32)

    A, B = 0, 1
    y_args = [
        (sbuf.at[0], relay.at[0], y_send.at[0], y_recv.at[0], y_up),
        (sbuf.at[1], relay.at[1], y_send.at[1], y_recv.at[1], y_dn),
        (sbuf.at[2], fin.at[0, B], y_send.at[2], y_recv.at[2], y_up),
        (sbuf.at[3], fin.at[1, A], y_send.at[3], y_recv.at[3], y_dn),
        (sbuf.at[4], fin.at[0, A], y_send.at[4], y_recv.at[4], y_up),
        (sbuf.at[5], fin.at[1, B], y_send.at[5], y_recv.at[5], y_dn),
    ]

    def y_go(i, value):
        sbuf[i] = value.astype(BF)
        remote(*y_args[i]).start()

    y_go(0, chip_sum(A, 0))
    y_go(1, chip_sum(B, 0))
    y_go(3, chip_sum(A, 2))
    y_go(2, chip_sum(B, 1))
    up = chip_sum(A, 1)
    arrived(relay.at[0], y_recv.at[0])
    y_go(4, up + relay[0].astype(F32))
    dn = chip_sum(B, 2)
    arrived(relay.at[1], y_recv.at[1])
    y_go(5, dn + relay[1].astype(F32))

    arrived(fin.at[0, B], y_recv.at[2])
    arrived(fin.at[1, A], y_recv.at[3])
    arrived(fin.at[0, A], y_recv.at[4])
    arrived(fin.at[1, B], y_recv.at[5])
    for h in range(2):
        whole = chip_sum(h, 3) + fin[0, h].astype(F32) + fin[1, h].astype(F32)
        out[:, 2048 * h:2048 * h + 2048] = whole.astype(BF)

    for a in ret_args:
        sent_any(*a)
    for h in range(2):
        for k in range(4):
            remote(*pd_args(h, k)).wait_send()
    for a in y_args:
        remote(*a).wait_send()


def body(tokens, norm_gain, w_pool_in, w_query, w_key, w_value, pool_mix, pool_scale, lam, head_gain,
         pool_proj, attn_proj):
    sd = jax.ShapeDtypeStruct
    kv, q, pool_in, lam_tile = pl.pallas_call(
        project_kernel,
        out_shape=(sd((2, 2, 512, 128), BF), sd((2, ROWS, 128), BF), sd((ROWS, 256), BF), sd((2, 8, 128), F32)),
        in_specs=[ANY, VM, ANY, ANY, ANY, ANY, SM],
        out_specs=(VM, VM, VM, VM),
        scratch_shapes=[
            pltpu.VMEM((ROWS, WIDE), BF), pltpu.VMEM((ROWS, WIDE), BF), pltpu.VMEM((4, WIDE, 256), BF),
            pltpu.SemaphoreType.DMA((4,)), pltpu.SemaphoreType.DMA((4,)),
        ],
        compiler_params=pltpu.CompilerParams(vmem_limit_bytes=40 << 20),
        name="project",
    )(tokens, norm_gain.reshape(1, WIDE), w_key, w_value, w_query, w_pool_in, lam)

    dma = pltpu.SemaphoreType.DMA
    return pl.pallas_call(
        mixer_kernel,
        out_shape=sd((64, WIDE), BF),
        in_specs=[VM, VM, VM, VM, VM, VM, VM, ANY, ANY],
        out_specs=VM,
        scratch_shapes=[
            pltpu.VMEM((4, 2, 4, 512, 128), BF),
            pltpu.VMEM((2, ROWS, 128), BF),
            pltpu.VMEM((2, 2, ROWS, 128), BF),
            pltpu.VMEM((2, 8, 128), F32),
            pltpu.VMEM((16, 256), BF),
            pltpu.VMEM((2, 2, 128, ROWS), F32),
            pltpu.VMEM((2, 2, 1, ROWS), F32),
            pltpu.VMEM((2, 2, 1, ROWS), F32),
            pltpu.VMEM((2, ROWS, 128), BF),
            pltpu.VMEM((2, ROWS, 128), BF),
            pltpu.VMEM((ROWS, 256), BF),
            pltpu.VMEM((512, WIDE), BF),
            pltpu.VMEM((2, 8, 64, 2048), BF),
            pltpu.VMEM((2, 4, 64, 2048), BF),
            pltpu.VMEM((6, 64, 2048), BF),
            pltpu.VMEM((2, 64, 2048), BF),
            pltpu.VMEM((2, 2, 64, 2048), BF),
            dma((2,)), dma((2, 2)), dma((4, 2, 4)), dma((2,)), dma((2,)), dma((2,)), dma((2,)),
            dma, dma, dma((2, 4)), dma((2, 4)), dma((4, 4)), dma((2,)), dma((2,)),
            dma((2, 4)), dma((2, 4)), dma((6,)), dma((6,)),
        ],
        compiler_params=pltpu.CompilerParams(vmem_limit_bytes=60 << 20, collective_id=0, has_side_effects=True),
        name="mixer",
    )(kv, q, pool_in, lam_tile, pool_mix.reshape(256, 64), pool_scale.reshape(1, 256), head_gain.reshape(1, 128),
      pool_proj, attn_proj)


def solution(mesh):
    return jax.shard_map(
        body,
        mesh=mesh,
        in_specs=(P("sp", None), P(), P(None, "tp"), P(None, "tp"), P(None, "tp"), P(None, "tp"),
                  P("tp", None, None), P("tp"), P("tp"), P(), P("tp", None), P("tp", None)),
        out_specs=P(("sp", "tp"), None),
        check_vma=False,
    )
```

time: 266 us -> 110 us (0.41)
  waiting for transfers between devices: 157 us -> 0 us
  Pallas kernels: 0 us -> 94.5 us
  matrix products: 36.1 us -> 0 us
  other arithmetic: 16.5 us -> 0 us
  between operations: 13.7 us -> 0.04 us
  loops' own time: 12 us -> 0 us
  local copies, waits for them, and re-layouts: 25.9 us -> 14.6 us
  starting transfers between devices: 3.62 us -> 0 us
    reduce_scatter x1 -> x0, waiting for transfers between devices: 96.2 us -> none  [body(): lax.psum_scatter((term + jnp.dot(attn_out, attn_proj, preferred_element_t...]
    pallas_call x0 -> x2, Pallas kernels: none -> 94.5 us  [the longest x1 79 us: body(): pl.pallas_call(mixer_kernel, out_shape=sd((64, WIDE), BF), in_specs=[VM,...]
    all_gather x1 -> x0, waiting for transfers between devices: 60.6 us -> none  [sent_together(): whole = lax.all_gather(both, axis, axis=dim, tiled=True)]
    dot_general x17 -> x0, matrix products: 36.1 us -> none  [the longest x5 9.04 us: attend_block(): jnp.einsum('hmqk,khe->hmqe', probs.astype(jnp.bfloat16), values, preferre...]
    dynamic_slice x21 -> x0, local copies, waits for them, and re-layouts: 16.1 us -> none  [the longest x16 9.38 us: sweep(): lax.scan(one, carry, jnp.arange(count_rows // block, dtype=jnp.int32))]
    unnamed x20 -> x23, local copies, waits for them, and re-layouts: 2.17 us -> 14.6 us
    another operation x17 -> x0, loops' own time: 12 us -> none  [the longest x1 11.4 us: sweep(): lax.scan(one, carry, jnp.arange(count_rows // block, dtype=jnp.int32))]
    reduce_sum x7 -> x0, other arithmetic: 8.62 us -> none  [the longest x5 5.21 us: attend_block(): weight_sum = weight_sum * shrink + jnp.sum(probs, axis=-1)]
  transfers between devices with their start and end apart: 3 -> 0, of which waited for: 2 -> 0; matrix products, arithmetic and copies ran while one was open for 6% -> 0% of each run, Pallas kernels for 0% -> 0%
where the time goes in v1:
time: 110 us; the launch traced here: 109 us
  Pallas kernels  94.5 us (86%)
  local copies, waits for them, and re-layouts  14.6 us (13%)
    pallas_call x1, Pallas kernels, body(): pl.pallas_call(mixer_kernel, out_shape=sd((64, WIDE), BF), in_specs=[VM,...  79 us
    pallas_call x1, Pallas kernels, body(): pl.pallas_call(project_kernel, out_shape=(sd((2, 2, 512, 128), BF), sd((2...  15.5 us
    unnamed x23, local copies, waits for them, and re-layouts  14.6 us

profile of v1, /device:TPU:32, one launch (start us, length us, event | category | flops | bytes accessed | tf_op | source)
XLA Modules:
  0.0 109.1 jit_solution(14815387471783890664)
XLA Ops:
  0.0 0.0 copy-start
  0.0 2.2 %copy-done = bf16[512,4096]{1,0:T(8,128)(2,1)S(1)} copy-done((bf16[512,4096]{1,0:T(8,128)(2,1)S(1)}, bf16[512,4096]{1,0:T(8,128)(2,1)}, u32[]{:S(2)}) %copy-start) | copy-done | bytes 4194328
  2.2 0.0 copy-start.1
  2.2 1.6 %copy-done.1 = bf16[4096,256]{1,0:T(8,128)(2,1)S(1)} copy-done((bf16[4096,256]{1,0:T(8,128)(2,1)S(1)}, bf16[4096,256]{1,0:T(8,128)(2,1)}, u32[]{:S(2)}) %copy-start.1) | copy-done | bytes 2097176
  3.8 0.0 copy-start.2
  3.8 1.6 %copy-done.2 = bf16[4096,256]{1,0:T(8,128)(2,1)S(1)} copy-done((bf16[4096,256]{1,0:T(8,128)(2,1)S(1)}, bf16[4096,256]{1,0:T(8,128)(2,1)}, u32[]{:S(2)}) %copy-start.2) | copy-done | bytes 2097176
  5.4 0.0 copy-start.3
  5.4 1.6 %copy-done.3 = bf16[4096,256]{1,0:T(8,128)(2,1)S(1)} copy-done((bf16[4096,256]{1,0:T(8,128)(2,1)S(1)}, bf16[4096,256]{1,0:T(8,128)(2,1)}, u32[]{:S(2)}) %copy-start.3) | copy-done | bytes 2097176
  7.0 0.0 copy-start.4
  7.0 1.6 %copy-done.4 = bf16[4096,256]{1,0:T(8,128)(2,1)S(1)} copy-done((bf16[4096,256]{1,0:T(8,128)(2,1)S(1)}, bf16[4096,256]{1,0:T(8,128)(2,1)}, u32[]{:S(2)}) %copy-start.4) | copy-done | bytes 2097176
  8.6 0.0 copy-start.8
  8.6 0.7 copy-done.8
  9.3 0.0 copy-start.10
  9.3 0.7 copy-done.10
  9.9 15.5 %project.1 = (bf16[2,2,512,128]{3,2,1,0:T(8,128)(2,1)S(1)}, bf16[2,512,128]{2,1,0:T(8,128)(2,1)S(1)}, bf16[512,256]{1,0:T(8,128)(2,1)S(1)}, f32[2,8,128]{2,1,0:T(8,128)S(1)}) custom-call(bf16[512,4096]{1,0:T(8,128)(2,1)S(1)} %copy-done, f32[1,4096]{1,0:T(1,128)S(1)} %bitcast.4, bf16[4096,256]{1,0:T(8,128)(2,1)S(1)} %copy-done.1, ...), custom_call_target="tpu_custom_call" | custom-call | tf_op jit(solution)/shard_map/project/pallas_call | solution.py:390
  25.5 0.0 copy-start.5
  25.5 0.8 copy-done.5
  26.2 0.0 copy-start.6
  26.3 0.7 copy-done.6
  27.0 0.0 copy-start.7
  27.0 0.7 copy-done.7
  27.7 0.0 copy-start.9
  27.7 0.6 copy-done.9
  28.2 79.0 %mixer.1 = bf16[64,4096]{1,0:T(8,128)(2,1)} custom-call(bf16[2,2,512,128]{3,2,1,0:T(8,128)(2,1)} %copy-done.5, bf16[2,512,128]{2,1,0:T(8,128)(2,1)} %copy-done.6, bf16[512,256]{1,0:T(8,128)(2,1)} %copy-done.7, f32[2,8,128]{2,1,0:T(8,128)} %copy-done.9, bf16[256,64]{1,0:T(8,128)(2,1)} %bitcast.5, f32[1,256]{1,0:T(1,128)} %bitcast.6, f32[1,128]{1,0:T(1,128)} %bitcast.7, ...), custom_call_target="tpu_custom_call" | custom-call | tf_op jit(solution)/shard_map/mixer/pallas_call | solution.py:404
  107.2 1.9 %copy.14 = bf16[64,4096]{1,0:T(8,128)(2,1)} copy(bf16[64,4096]{1,0:T(8,128)(2,1)} %mixer.1) | data formatting | bytes 1048576
Async XLA Ops:
  0.0 2.2 %copy-start = (bf16[512,4096]{1,0:T(8,128)(2,1)S(1)}, bf16[512,4096]{1,0:T(8,128)(2,1)}, u32[]{:S(2)}) copy-start(bf16[512,4096]{1,0:T(8,128)(2,1)} %tok.1) | copy-start | bytes 12582916
  2.2 1.6 %copy-start.1 = (bf16[4096,256]{1,0:T(8,128)(2,1)S(1)}, bf16[4096,256]{1,0:T(8,128)(2,1)}, u32[]{:S(2)}) copy-start(bf16[4096,256]{1,0:T(8,128)(2,1)} %w_k.1) | copy-start | bytes 6291460
  3.8 1.6 %copy-start.2 = (bf16[4096,256]{1,0:T(8,128)(2,1)S(1)}, bf16[4096,256]{1,0:T(8,128)(2,1)}, u32[]{:S(2)}) copy-start(bf16[4096,256]{1,0:T(8,128)(2,1)} %w_v.1) | copy-start | bytes 6291460
  5.4 1.6 %copy-start.3 = (bf16[4096,256]{1,0:T(8,128)(2,1)S(1)}, bf16[4096,256]{1,0:T(8,128)(2,1)}, u32[]{:S(2)}) copy-start(bf16[4096,256]{1,0:T(8,128)(2,1)} %w_q.1) | copy-start | bytes 6291460
  7.0 1.6 %copy-start.4 = (bf16[4096,256]{1,0:T(8,128)(2,1)S(1)}, bf16[4096,256]{1,0:T(8,128)(2,1)}, u32[]{:S(2)}) copy-start(bf16[4096,256]{1,0:T(8,128)(2,1)} %w_p.1) | copy-start | bytes 6291460
  8.6 0.7 copy-start.8
  9.3 0.7 copy-start.10
  25.5 0.8 copy-start.5
  26.2 0.7 copy-start.6
  27.0 0.7 copy-start.7
  27.7 0.6 copy-start.9

commit v2 on v1

v2 whole, which is shorter than its diff:
```python
import jax
import jax.numpy as jnp
from jax import lax
from jax.experimental import pallas as pl
from jax.experimental.pallas import tpu as pltpu
from jax.sharding import PartitionSpec as P

EPS = 1e-6
NEG = -1e30
LOG2E = 1.4426950408889634
ROWS = 512
WIDE = 4096
SEG = 64
BF = jnp.bfloat16
F32 = jnp.float32
MESH_ID = pl.DeviceIdType.MESH
ANY = pl.BlockSpec(memory_space=pl.ANY)
VM = pl.BlockSpec(memory_space=pltpu.VMEM)
SM = pl.BlockSpec(memory_space=pltpu.SMEM)


def mixer_kernel(tok, gain, w_k, w_v, w_q, w_p, lam, pool_mix, pool_scale, head_gain, pool_proj, attn_proj,
                 out,
                 raw, normed, wts, kv_in, q_in, pool_in, lam_in, kv, qraw, qcat, lamb, rim, acc, top, den, sbank_a, sbank_b, ao, ab, pooled, w_out, pbuf, dbuf, sbuf, relay, fin,
                 tok_sem, w_sem, a2a_send, kv_recv, q_send, q_recv, lam_send, lam_recv, rim_send, rim_recv,
                 zp_send, zm_send, dd_send, ret_send, ret_recv, pd_send, pd_recv, y_send, y_recv):
    sbank = (sbank_a, sbank_b)
    sp = lax.axis_index("sp")
    tp = lax.axis_index("tp")
    z, x = lax.div(sp, 4), lax.rem(sp, 4)
    y, c = lax.div(tp, 2), lax.rem(tp, 2)

    def wrap(i):
        return lax.rem(i + 4, 4)

    def dev(zz, xx, cc):
        return (zz * 4 + xx, y * 2 + cc)

    me = (sp, tp)

    def is_me(d):
        return (d[0] == sp) & (d[1] == tp)

    core_src = lax.div(x, 2)
    odd_row = lax.rem(z, 2) == 1
    zq = jnp.where(odd_row, 3 - x, x)
    cq = jnp.where((z == 0) | (z == 3), 0, 1)
    sq = lax.div(z, 2)
    qb = [jnp.where(c == 0, z, 7 - z), jnp.where(c == 0, 15 - z, 8 + z)]
    partner = dev(z, x, 1 - c)
    z_up, z_dn = dev(wrap(z + 1), x, c), dev(wrap(z - 1), x, c)
    y_up = (sp, wrap(y + 1) * 2 + c)
    y_dn = (sp, wrap(y - 1) * 2 + c)
    nxt = (lax.rem(sp + 1, 16), tp)
    prv = (lax.rem(sp + 15, 16), tp)
    a2a_dst = [[dev(z, 2 * c + hh, hf) for hf in range(2)] for hh in range(2)]
    q_dst = [dev(zq, 2 * c + hh, cq) for hh in range(2)]
    q_src = [dev(lax.div(qb[s], 4), lax.rem(qb[s], 4), core_src) for s in range(2)]

    def load(src, dst, sem):
        cp = pltpu.make_async_copy(src, dst, sem)
        cp.start()
        return cp

    tok_loads = [load(tok.at[pl.ds(r * 128, 128)], raw.at[pl.ds(r * 128, 128)], tok_sem.at[r]) for r in range(4)]
    in_loads = [load(w, wts.at[i], w_sem.at[i]) for i, w in enumerate((w_k, w_v, w_q, w_p))]
    w_loads = [load(pool_proj, w_out.at[pl.ds(0, 256)], w_sem.at[4]),
               load(attn_proj, w_out.at[pl.ds(256, 256)], w_sem.at[5])]

    barrier = pltpu.get_barrier_semaphore()

    def greet(d):
        pl.semaphore_signal(barrier, inc=1, device_id=d, device_id_type=MESH_ID)

    greeted = [dev(z, xk, core_src) for xk in range(4)] + q_src + q_dst + [z_up, z_dn, partner, y_up, y_dn, prv]
    for d in greeted:
        greet(d)

    def remote(src, dst, ssem, rsem, d):
        return pltpu.make_async_remote_copy(src_ref=src, dst_ref=dst, send_sem=ssem, recv_sem=rsem,
                                            device_id=d, device_id_type=MESH_ID)

    def send_any(src, dst, ssem, rsem, d):
        @pl.when(is_me(d))
        def _():
            pltpu.make_async_copy(src, dst, rsem).start()

        @pl.when(jnp.logical_not(is_me(d)))
        def _():
            remote(src, dst, ssem, rsem, d).start()

    def sent_any(src, dst, ssem, rsem, d):
        @pl.when(jnp.logical_not(is_me(d)))
        def _():
            remote(src, dst, ssem, rsem, d).wait_send()

    def arrived(dst, rsem):
        pltpu.make_async_copy(dst, dst, rsem).wait()

    for hh in range(2):
        lam_in[hh] = jnp.full((8, 128), lam[hh], F32)
    with jax.named_scope("norm"):
        for r in range(4):
            tok_loads[r].wait()

            @pl.loop(0, 8, unroll=4)
            def _(i):
                rows = pl.ds(pl.multiple_of(r * 128 + i * 16, 16), 16)
                wide = raw[rows].astype(F32)
                scale = lax.rsqrt(jnp.mean(wide * wide, axis=-1, keepdims=True) + EPS)
                normed[rows] = (wide * scale * gain[...]).astype(BF)

    def product(i):
        return jnp.dot(normed[...], wts[i], preferred_element_type=F32)

    with jax.named_scope("keys_values"):
        in_loads[0].wait()
        in_loads[1].wait()
        keys = product(0).astype(BF)
        values = product(1)
        for hh in range(2):
            for hf in range(2):
                kv_in[hh, hf, 0:256] = keys[256 * hf:256 * hf + 256, 128 * hh:128 * hh + 128]
                for j in range(2):
                    first = 256 * hf + 128 * j
                    tile = values[first:first + 128, 128 * hh:128 * hh + 128]
                    kv_in[hh, hf, 256 + 128 * j:384 + 128 * j] = tile.T.astype(BF)

    pl.semaphore_wait(barrier, len(greeted))

    a2a_args = []
    for hh in range(2):
        for hf in range(2):
            a2a_args.append((kv_in.at[hh, hf], kv.at[z, hf, x], a2a_send.at[hh, hf], kv_recv.at[0, hf, x],
                             a2a_dst[hh][hf]))
    for a in a2a_args:
        send_any(*a)

    def dd_args(rel, xk):
        piece = kv.at[wrap(z + rel), c, xk]
        return (piece, piece, dd_send.at[rel, xk], kv_recv.at[rel, c, xk], partner)

    def up_args(rel, xk):
        piece = kv.at[wrap(z + rel), c, xk]
        return (piece, piece, zp_send.at[rel & 1, xk], kv_recv.at[(rel + 3) % 4, c, xk], z_up)

    def dn_args(rel, xk):
        piece = kv.at[wrap(z + rel), c, xk]
        return (piece, piece, zm_send.at[rel & 1, xk], kv_recv.at[(rel + 1) % 4, c, xk], z_dn)

    def mine(rel, xk):
        arrived(kv.at[wrap(z + rel), c, xk], kv_recv.at[rel, c, xk])

    def at(off):
        return lax.rem(x + off, 4)

    def go(args):
        remote(*args).start()

    mine(0, at(0))
    go(up_args(0, at(0)))
    go(dn_args(0, at(0)))
    go(dd_args(0, at(0)))

    with jax.named_scope("query_pool"):
        in_loads[2].wait()
        in_loads[3].wait()
        query = product(2) * (0.125 * LOG2E)
        pool_in[...] = product(3).astype(BF)
        for hh in range(2):
            q_in[hh] = query[:, 128 * hh:128 * hh + 128].T.astype(BF)
    rim_args = (pool_in.at[pl.ds(ROWS - 16, 16)], rim, rim_send, rim_recv, nxt)
    go(rim_args)
    q_args = []
    for hh in range(2):
        q_args.append((q_in.at[hh], qraw.at[sq], q_send.at[hh], q_recv.at[sq], q_dst[hh]))
        q_args.append((lam_in.at[hh], lamb.at[sq], lam_send.at[hh], lam_recv.at[sq], q_dst[hh]))
    for a in q_args:
        send_any(*a)

    with jax.named_scope("own_near"):
        mine(0, at(1))
        go(up_args(0, at(1)))
        go(dd_args(0, at(1)))
        mine(0, at(3))
        go(dn_args(0, at(3)))
        go(up_args(0, at(3)))
        go(dd_args(0, at(3)))

    with jax.named_scope("pooling"):
        arrived(rim, rim_recv)
        edge = jnp.where(sp == 0, 0.0, rim[...].astype(F32))
        own = pool_in[...].astype(F32)
        lane = lax.broadcasted_iota(jnp.int32, (1, 128), 1)
        totals = []
        for side in range(2):
            cols = slice(128 * side, 128 * side + 128)
            line = jnp.concatenate([edge[:, cols], own[:, cols]], axis=0)
            s2 = line + pltpu.roll(line, 1, 0)
            s4 = s2 + pltpu.roll(s2, 2, 0)
            if side == 0:
                totals.append(jnp.where(lane < 64, s2, s4)[16:])
            else:
                s8 = s4 + pltpu.roll(s4, 4, 0)
                s16 = s8 + pltpu.roll(s8, 8, 0)
                totals.append(jnp.where(lane < 64, s8, s16)[16:])
        total = jnp.concatenate(totals, axis=1)
        lane = lax.broadcasted_iota(jnp.int32, (1, 256), 1)
        window = jnp.where(lane < 64, 2, jnp.where(lane < 128, 4, jnp.where(lane < 192, 8, 16)))
        position = sp * ROWS + lax.broadcasted_iota(jnp.int32, (16, 256), 0)
        early = total[:16] / jnp.minimum(position + 1, window).astype(F32)
        later = total[16:] * (1.0 / window.astype(F32))
        mixed_in = (jnp.concatenate([early, later], axis=0) - own).astype(BF)
        spread = (lax.rem(lax.broadcasted_iota(jnp.int32, (64, 256), 1), 64)
                  == lax.broadcasted_iota(jnp.int32, (64, 256), 0)).astype(F32).astype(BF)
        wide_mix = jnp.dot(pool_mix[...], spread, preferred_element_type=F32)
        same = (lax.div(lax.broadcasted_iota(jnp.int32, (256, 256), 0), 64)
                == lax.div(lax.broadcasted_iota(jnp.int32, (256, 256), 1), 64))
        block_mix = jnp.where(same, wide_mix, 0.0).astype(BF)
        grouped = jnp.dot(mixed_in, block_mix, preferred_element_type=F32)
        pooled[...] = (grouped * pool_scale[...]).astype(BF)

    with jax.named_scope("own_far"):
        mine(0, at(2))
        go(dn_args(0, at(2)))
        go(up_args(0, at(2)))
        go(dd_args(0, at(2)))
        go(dn_args(0, at(1)))

    with jax.named_scope("queries"):
        for s in range(2):
            arrived(qraw.at[s], q_recv.at[s])
            arrived(lamb.at[s], lam_recv.at[s])
            q = qraw[s]
            zero = jnp.zeros((64, ROWS), BF)
            qcat[s, 0] = jnp.concatenate([q[:64], zero], axis=0)
            qcat[s, 1] = jnp.concatenate([zero, q[64:]], axis=0)
            for m in range(2):
                top[s, m] = jnp.full((1, ROWS), NEG, F32)
                den[s, m] = jnp.zeros((1, ROWS), F32)
                acc[s, m] = jnp.zeros((128, ROWS), F32)

    def attend(zk, xk, first, masked):
        halves = [kv[zk, hf, xk] for hf in range(2)]
        keys = jnp.concatenate([h[:256] for h in halves], axis=0)
        vals = jnp.concatenate([h[256 + 128 * j:384 + 128 * j] for h in halves for j in range(2)], axis=1)
        tiles = [(s, m) for s in range(first, 2) for m in range(2)]

        def score(n):
            s, m = tiles[n]
            scores = jnp.dot(keys, qcat[s, m], preferred_element_type=F32)
            if masked and s == first:
                allowed = (lax.div(lax.broadcasted_iota(jnp.int32, (ROWS, ROWS), 0), SEG)
                           <= lax.div(lax.broadcasted_iota(jnp.int32, (ROWS, ROWS), 1), SEG))
                scores = jnp.where(allowed, scores, NEG)
            sbank[n % 2][...] = scores

        score(0)
        for n, (s, m) in enumerate(tiles):
            if n + 1 < len(tiles):
                score(n + 1)
            scores = sbank[n % 2][...]
            old = top[s, m]
            new = jnp.maximum(old, jnp.max(scores, axis=0, keepdims=True))
            probs = jnp.exp2(scores - new)
            shrink = jnp.exp2(old - new)
            top[s, m] = new
            den[s, m] = den[s, m] * shrink + jnp.sum(probs, axis=0, keepdims=True)
            acc[s, m] = acc[s, m] * shrink + jnp.dot(vals, probs.astype(BF), preferred_element_type=F32)

    def visit(rel, xk):
        zk = wrap(z + rel)
        arrived(kv.at[zk, 1 - c, xk], kv_recv.at[rel, 1 - c, xk])
        block = zk * 4 + xk

        @pl.when(block < qb[0])
        def _():
            attend(zk, xk, 0, False)

        @pl.when(block == qb[0])
        def _():
            attend(zk, xk, 0, True)

        @pl.when((block > qb[0]) & (block < qb[1]))
        def _():
            attend(zk, xk, 1, False)

        @pl.when(block == qb[1])
        def _():
            attend(zk, xk, 1, True)

    below, above = (0, 1, 3, 2), (0, 3, 2, 1)
    plan = ([(0, o) for o in below] + [p for i in range(4) for p in ((3, below[i]), (1, above[i]))]
            + [(2, o) for o in (0, 3, 1, 2)])

    def near(i):
        mine(3, at(below[i]))
        if i < 2:
            go(up_args(3, at(below[i])))
        go(dd_args(3, at(below[i])))
        mine(1, at(above[i]))
        if i in (1, 2):
            go(dn_args(1, at(above[i])))
        go(dd_args(1, at(above[i])))

    def far(i):
        for off in ((0, 3), (1, 2))[i]:
            mine(2, at(off))
            go(dd_args(2, at(off)))

    def pick(v, values):
        out_value = jnp.int32(values[0])
        for i, value in enumerate(values):
            if i:
                out_value = jnp.where(v == i, value, out_value)
        return out_value

    service = {0: (near, 0), 2: (near, 1), 5: (near, 2), 7: (near, 3), 10: (far, 0), 12: (far, 1)}

    with jax.named_scope("attend"):
        @pl.loop(0, 16)
        def _(v):
            for when, (serve, i) in service.items():
                @pl.when(v == when)
                def _():
                    serve(i)

            visit(pick(v, [p[0] for p in plan]), at(pick(v, [p[1] for p in plan])))

    ret_args = []
    with jax.named_scope("finish"):
        for s in range(2):
            o1 = acc[s, 0] / den[s, 0]
            o2 = acc[s, 1] / den[s, 1]
            blend = o1 - lamb[s][0:1, 0:1] * o2
            scaled = blend * lax.rsqrt(jnp.mean(blend * blend, axis=0, keepdims=True) + EPS)
            ao[s] = (scaled.T * head_gain[...] * 0.8).astype(BF)
            mine_h = lax.rem(x, 2)
            a = (ao.at[s], ab.at[mine_h], ret_send.at[s], ret_recv.at[mine_h], q_src[s])
            send_any(*a)
            ret_args.append(a)

    with jax.named_scope("drain"):
        remote(*rim_args).wait_send()
        for a in a2a_args + q_args:
            sent_any(*a)
        for off in range(4):
            remote(*up_args(0, at(off))).wait_send()
            remote(*dn_args(0, at(off))).wait_send()
            for rel in range(4):
                remote(*dd_args(rel, at(off))).wait_send()
        for i in range(2):
            remote(*up_args(3, at(below[i]))).wait_send()
            remote(*dn_args(1, at(above[i + 1]))).wait_send()

    for cp in w_loads:
        cp.wait()
    with jax.named_scope("home"):
        for hh in range(2):
            arrived(ab.at[hh], ret_recv.at[hh])

    order = [wrap(y + 2), wrap(y + 1), wrap(y - 1), y]

    def pd_args(h, k):
        return (pbuf.at[h, 2 * order[k] + 1 - c], dbuf.at[h, k], pd_send.at[h, k], pd_recv.at[h, k], partner)

    with jax.named_scope("project"):
        for h in range(2):
            feats = jnp.concatenate([pooled[...], ab[0], ab[1]], axis=1)
            term = jnp.dot(feats, w_out[:, 2048 * h:2048 * h + 2048], preferred_element_type=F32)
            pbuf[h] = term.astype(BF).reshape(8, 64, 2048)
            for k in range(4):
                go(pd_args(h, k))

    def chip_sum(h, k):
        arrived(dbuf.at[h, k], pd_recv.at[h, k])
        return pbuf[h, 2 * order[k] + c].astype(F32) + dbuf[h, k].astype(F32)

    A, B = 0, 1
    y_args = [
        (sbuf.at[0], relay.at[0], y_send.at[0], y_recv.at[0], y_up),
        (sbuf.at[1], relay.at[1], y_send.at[1], y_recv.at[1], y_dn),
        (sbuf.at[2], fin.at[0, B], y_send.at[2], y_recv.at[2], y_up),
        (sbuf.at[3], fin.at[1, A], y_send.at[3], y_recv.at[3], y_dn),
        (sbuf.at[4], fin.at[0, A], y_send.at[4], y_recv.at[4], y_up),
        (sbuf.at[5], fin.at[1, B], y_send.at[5], y_recv.at[5], y_dn),
    ]

    def y_go(i, value):
        sbuf[i] = value.astype(BF)
        remote(*y_args[i]).start()

    with jax.named_scope("y_first"):
        y_go(0, chip_sum(A, 0))
        y_go(1, chip_sum(B, 0))
        y_go(3, chip_sum(A, 2))
        y_go(2, chip_sum(B, 1))
    with jax.named_scope("y_relay"):
        up = chip_sum(A, 1)
        arrived(relay.at[0], y_recv.at[0])
        y_go(4, up + relay[0].astype(F32))
        dn = chip_sum(B, 2)
        arrived(relay.at[1], y_recv.at[1])
        y_go(5, dn + relay[1].astype(F32))

    with jax.named_scope("y_last"):
        arrived(fin.at[0, B], y_recv.at[2])
        arrived(fin.at[1, A], y_recv.at[3])
        arrived(fin.at[0, A], y_recv.at[4])
        arrived(fin.at[1, B], y_recv.at[5])
        for h in range(2):
            whole = chip_sum(h, 3) + fin[0, h].astype(F32) + fin[1, h].astype(F32)
            out[:, 2048 * h:2048 * h + 2048] = whole.astype(BF)

    for a in ret_args:
        sent_any(*a)
    for h in range(2):
        for k in range(4):
            remote(*pd_args(h, k)).wait_send()
    for a in y_args:
        remote(*a).wait_send()


def body(tokens, norm_gain, w_pool_in, w_query, w_key, w_value, pool_mix, pool_scale, lam, head_gain,
         pool_proj, attn_proj):
    sd = jax.ShapeDtypeStruct
    dma = pltpu.SemaphoreType.DMA
    return pl.pallas_call(
        mixer_kernel,
        out_shape=sd((64, WIDE), BF),
        in_specs=[ANY, VM, ANY, ANY, ANY, ANY, SM, VM, VM, VM, ANY, ANY],
        out_specs=VM,
        scratch_shapes=[
            pltpu.VMEM((ROWS, WIDE), BF),
            pltpu.VMEM((ROWS, WIDE), BF),
            pltpu.VMEM((4, WIDE, 256), BF),
            pltpu.VMEM((2, 2, 512, 128), BF),
            pltpu.VMEM((2, 128, ROWS), BF),
            pltpu.VMEM((ROWS, 256), BF),
            pltpu.VMEM((2, 8, 128), F32),
            pltpu.VMEM((4, 2, 4, 512, 128), BF),
            pltpu.VMEM((2, 128, ROWS), BF),
            pltpu.VMEM((2, 2, 128, ROWS), BF),
            pltpu.VMEM((2, 8, 128), F32),
            pltpu.VMEM((16, 256), BF),
            pltpu.VMEM((2, 2, 128, ROWS), F32),
            pltpu.VMEM((2, 2, 1, ROWS), F32),
            pltpu.VMEM((2, 2, 1, ROWS), F32),
            pltpu.VMEM((ROWS, ROWS), F32),
            pltpu.VMEM((ROWS, ROWS), F32),
            pltpu.VMEM((2, ROWS, 128), BF),
            pltpu.VMEM((2, ROWS, 128), BF),
            pltpu.VMEM((ROWS, 256), BF),
            pltpu.VMEM((512, WIDE), BF),
            pltpu.VMEM((2, 8, 64, 2048), BF),
            pltpu.VMEM((2, 4, 64, 2048), BF),
            pltpu.VMEM((6, 64, 2048), BF),
            pltpu.VMEM((2, 64, 2048), BF),
            pltpu.VMEM((2, 2, 64, 2048), BF),
            dma((4,)), dma((6,)), dma((2, 2)), dma((4, 2, 4)), dma((2,)), dma((2,)), dma((2,)), dma((2,)),
            dma, dma, dma((2, 4)), dma((2, 4)), dma((4, 4)), dma((2,)), dma((2,)),
            dma((2, 4)), dma((2, 4)), dma((6,)), dma((6,)),
        ],
        compiler_params=pltpu.CompilerParams(vmem_limit_bytes=67043328, collective_id=0, has_side_effects=True),
        name="mixer",
    )(tokens, norm_gain.reshape(1, WIDE), w_key, w_value, w_query, w_pool_in, lam, pool_mix.reshape(256, 64),
      pool_scale.reshape(1, 256), head_gain.reshape(1, 128), pool_proj, attn_proj)


def solution(mesh):
    return jax.shard_map(
        body,
        mesh=mesh,
        in_specs=(P("sp", None), P(), P(None, "tp"), P(None, "tp"), P(None, "tp"), P(None, "tp"),
                  P("tp", None, None), P("tp"), P("tp"), P(), P("tp", None), P("tp", None)),
        out_specs=P(("sp", "tp"), None),
        check_vma=False,
    )
```

time: 110 us -> 77.6 us (0.71)
  Pallas kernels: 94.5 us -> 75.6 us
  local copies, waits for them, and re-layouts: 14.6 us -> 1.87 us
    pallas_call x2 -> x1, Pallas kernels: 94.5 us -> 75.6 us  [body(): pl.pallas_call(mixer_kernel, out_shape=sd((64, WIDE), BF), in_specs=[ANY,...]
    unnamed x23 -> x1, local copies, waits for them, and re-layouts: 14.6 us -> 1.87 us
where the time goes in v2:
time: 77.6 us; the launch traced here: 77.4 us
  Pallas kernels  75.6 us (97%)
  local copies, waits for them, and re-layouts  1.87 us (2%)
    pallas_call x1, Pallas kernels, body(): pl.pallas_call(mixer_kernel, out_shape=sd((64, WIDE), BF), in_specs=[ANY,...  75.6 us
    unnamed x1, local copies, waits for them, and re-layouts  1.87 us

profile of v2, /device:TPU:32, one launch (start us, length us, event | category | flops | bytes accessed | tf_op | source)
XLA Modules:
  0.0 77.4 jit_solution(14250347157433945829)
XLA Ops:
  0.0 75.6 %mixer.1 = bf16[64,4096]{1,0:T(8,128)(2,1)} custom-call(bf16[512,4096]{1,0:T(8,128)(2,1)} %tok.1, f32[1,4096]{1,0:T(1,128)} %bitcast.5, bf16[4096,256]{1,0:T(8,128)(2,1)} %w_k.1, bf16[4096,256]{1,0:T(8,128)(2,1)} %w_v.1, bf16[4096,256]{1,0:T(8,128)(2,1)} %w_q.1, bf16[4096,256]{1,0:T(8,128)(2,1)} %w_p.1, f32[2]{0:T(128)} %lam.1, bf16[256,64]{1,0:T(8,128)(2,1)} %bitcast.4, ...), custom_call_target="tpu_custom_call" | custom-call | tf_op jit(solution)/shard_map/mixer/pallas_call | solution.py:428
  75.6 1.9 %copy.14 = bf16[64,4096]{1,0:T(8,128)(2,1)} copy(bf16[64,4096]{1,0:T(8,128)(2,1)} %mixer.1) | data formatting | bytes 1048576

commit v3 on v2

v3 whole, which is shorter than its diff:
```python
import jax
import jax.numpy as jnp
from jax import lax
from jax.experimental import pallas as pl
from jax.experimental.pallas import tpu as pltpu
from jax.sharding import PartitionSpec as P

EPS = 1e-6
NEG = -1e30
LOG2E = 1.4426950408889634
ROWS = 512
WIDE = 4096
SEG = 64
BF = jnp.bfloat16
F32 = jnp.float32
MESH_ID = pl.DeviceIdType.MESH
OUTER = ((2, 3, 0, 1), (0, 3, 1, 2), (3, 2, 1, 0), (1, 0, 3, 2))
INNER = ((0, 2, 1, 3), (2, 1, 3, 0), (1, 0, 3, 2), (3, 2, 1, 0))


def pick(at, values):
    packed = sum(value << (2 * i) for i, value in enumerate(values))
    packed = packed - (1 << 32) if packed >= 1 << 31 else packed
    return lax.shift_right_logical(jnp.int32(packed), 2 * at) & 3


def flat(table):
    return [value for row in table for value in row]


def inverse(table):
    return [row.index(value) for row in table for value in range(4)]
ANY = pl.BlockSpec(memory_space=pl.ANY)
VM = pl.BlockSpec(memory_space=pltpu.VMEM)
SM = pl.BlockSpec(memory_space=pltpu.SMEM)


def mixer_kernel(tok, gain, w_k, w_v, w_q, w_p, lam, pool_mix, pool_scale, head_gain, pool_proj, attn_proj,
                 out,
                 raw, normed, wts, kv_in, q_in, pool_in, lam_in, kv, qraw, qcat, lamb, rim, acc, top, den, sbank_a, sbank_b, smax, x_relay, ao, ab, pooled, w_out, pbuf, dbuf, sbuf, relay, fin,
                 tok_sem, w_sem, x_recv, pass_send, a2a_send, kv_recv, q_send, q_recv, lam_send, lam_recv, rim_send, rim_recv,
                 zp_send, zm_send, dd_send, ret_send, ret_recv, pd_send, pd_recv, y_send, y_recv):
    sbank = (sbank_a, sbank_b)
    sp = lax.axis_index("sp")
    tp = lax.axis_index("tp")
    z, x = lax.div(sp, 4), lax.rem(sp, 4)
    y, c = lax.div(tp, 2), lax.rem(tp, 2)

    def wrap(i):
        return lax.rem(i + 4, 4)

    def dev(zz, xx, cc):
        return (zz * 4 + xx, y * 2 + cc)

    def at(off):
        return lax.rem(x + off, 4)

    me = (sp, tp)

    def is_me(d):
        return (d[0] == sp) & (d[1] == tp)

    core_src = lax.div(x, 2)
    outer_row = (z == 0) | (z == 3)
    place = jnp.where(z < 2, x, 3 - x)
    cq = jnp.where(outer_row, 0, 1)
    sq = lax.div(z, 2)
    a_here, b_here = pick(x * 4 + z, flat(OUTER)), pick(x * 4 + z, flat(INNER))
    qb = [jnp.where(c == 0, a_here, 4 + b_here), jnp.where(c == 0, 15 - a_here, 11 - b_here)]
    partner = dev(z, x, 1 - c)
    z_up, z_dn = dev(wrap(z + 1), x, c), dev(wrap(z - 1), x, c)
    y_up = (sp, wrap(y + 1) * 2 + c)
    y_dn = (sp, wrap(y - 1) * 2 + c)
    nxt = (lax.rem(sp + 1, 16), tp)
    prv = (lax.rem(sp + 15, 16), tp)
    a2a_dst = [[dev(z, 2 * c + hh, hf) for hf in range(2)] for hh in range(2)]
    q_dst = []
    for hh in range(2):
        spot = (2 * c + hh) * 4 + place
        q_dst.append(dev(jnp.where(outer_row, pick(spot, inverse(OUTER)), pick(spot, inverse(INNER))), 2 * c + hh, cq))
    q_src = [dev(lax.div(qb[s], 4), lax.rem(qb[s], 4), core_src) for s in range(2)]

    def load(src, dst, sem):
        cp = pltpu.make_async_copy(src, dst, sem)
        cp.start()
        return cp

    tok_loads = [load(tok.at[pl.ds(r * 128, 128)], raw.at[pl.ds(r * 128, 128)], tok_sem.at[r]) for r in range(4)]
    in_loads = []

    barrier = pltpu.get_barrier_semaphore()

    def greet(d):
        pl.semaphore_signal(barrier, inc=1, device_id=d, device_id_type=MESH_ID)

    behind, beyond = jnp.where(c == 0, at(3), at(1)), jnp.where(c == 0, at(1), at(3))
    greeted = [dev(z, at(off), core_src) for off in (0, 1, 3)] + [dev(z, behind, lax.div(beyond, 2)), dev(z, behind, c)]
    greeted = greeted + q_src + q_dst + [z_up, z_dn, partner, y_up, y_dn, prv]
    for d in greeted:
        greet(d)

    def remote(src, dst, ssem, rsem, d):
        return pltpu.make_async_remote_copy(src_ref=src, dst_ref=dst, send_sem=ssem, recv_sem=rsem,
                                            device_id=d, device_id_type=MESH_ID)

    def send_any(src, dst, ssem, rsem, d):
        @pl.when(is_me(d))
        def _():
            pltpu.make_async_copy(src, dst, rsem).start()

        @pl.when(jnp.logical_not(is_me(d)))
        def _():
            remote(src, dst, ssem, rsem, d).start()

    def sent_any(src, dst, ssem, rsem, d):
        @pl.when(jnp.logical_not(is_me(d)))
        def _():
            remote(src, dst, ssem, rsem, d).wait_send()

    def arrived(dst, rsem):
        pltpu.make_async_copy(dst, dst, rsem).wait()

    for hh in range(2):
        lam_in[hh] = jnp.full((8, 128), lam[hh], F32)
    with jax.named_scope("norm"):
        for r in range(4):
            tok_loads[r].wait()
            in_loads.append(load((w_q, w_k, w_v, w_p)[r], wts.at[r], w_sem.at[r]))

            @pl.loop(0, 8, unroll=4)
            def _(i):
                rows = pl.ds(pl.multiple_of(r * 128 + i * 16, 16), 16)
                wide = raw[rows].astype(F32)
                scale = lax.rsqrt(jnp.mean(wide * wide, axis=-1, keepdims=True) + EPS)
                normed[rows] = (wide * scale * gain[...]).astype(BF)

    def product(i):
        return jnp.dot(normed[...], wts[i], preferred_element_type=F32)

    def halves(i, finish_half):
        for r in range(2):
            rows = slice(256 * r, 256 * r + 256)
            finish_half(rows, jnp.dot(normed[rows], wts[i], preferred_element_type=F32))

    with jax.named_scope("query"):
        in_loads[0].wait()

        def query_half(rows, value):
            value = value * (0.125 * LOG2E)
            for hh in range(2):
                q_in[hh, :, rows] = value[:, 128 * hh:128 * hh + 128].T.astype(BF)

        halves(0, query_half)
    pl.semaphore_wait(barrier, len(greeted))
    q_args = []
    for hh in range(2):
        q_args.append((q_in.at[hh], qraw.at[sq], q_send.at[hh], q_recv.at[sq], q_dst[hh]))
        q_args.append((lam_in.at[hh], lamb.at[sq], lam_send.at[hh], lam_recv.at[sq], q_dst[hh]))
    for a in q_args:
        send_any(*a)

    with jax.named_scope("keys_values"):
        for i in range(1, 3):
            in_loads[i].wait()
        w_loads = [load(pool_proj, w_out.at[pl.ds(0, 256)], w_sem.at[4]),
                   load(attn_proj, w_out.at[pl.ds(256, 256)], w_sem.at[5])]
        keys = product(1).astype(BF)
        values = product(2)
        for hh in range(2):
            for hf in range(2):
                kv_in[hh, hf, 0:256] = keys[256 * hf:256 * hf + 256, 128 * hh:128 * hh + 128]
                for j in range(2):
                    first = 256 * hf + 128 * j
                    tile = values[first:first + 128, 128 * hh:128 * hh + 128]
                    kv_in[hh, hf, 256 + 128 * j:384 + 128 * j] = tile.T.astype(BF)

    a2a_args = []
    for hh in range(2):
        for hf in range(2):
            a2a_args.append((kv_in.at[hh, hf], kv.at[z, hf, x], a2a_send.at[hh, hf], kv_recv.at[0, hf, x],
                             a2a_dst[hh][hf]))

    def hop_args(hh, hf):
        return (kv_in.at[hh, hf], x_relay, a2a_send.at[hh, hf], x_recv, dev(z, at(1 if hf == 0 else 3), hf))

    for hh in range(2):
        is_across = wrap(2 * c + hh - x) == 2

        @pl.when(jnp.logical_not(is_across))
        def _():
            for hf in range(2):
                send_any(*a2a_args[2 * hh + hf])

    for hh in range(2):
        is_across = wrap(2 * c + hh - x) == 2

        @pl.when(is_across)
        def _():
            for hf in range(2):
                remote(*hop_args(hh, hf)).start()

    hop_from = jnp.where(c == 0, at(3), at(1))
    pass_args = (x_relay, kv.at[z, c, hop_from], pass_send, kv_recv.at[0, c, hop_from],
                 dev(z, jnp.where(c == 0, at(1), at(3)), c))


    def dd_args(rel, xk):
        piece = kv.at[wrap(z + rel), c, xk]
        return (piece, piece, dd_send.at[rel, xk], kv_recv.at[rel, c, xk], partner)

    def up_args(rel, xk):
        piece = kv.at[wrap(z + rel), c, xk]
        return (piece, piece, zp_send.at[rel & 1, xk], kv_recv.at[(rel + 3) % 4, c, xk], z_up)

    def dn_args(rel, xk):
        piece = kv.at[wrap(z + rel), c, xk]
        return (piece, piece, zm_send.at[rel & 1, xk], kv_recv.at[(rel + 1) % 4, c, xk], z_dn)

    def mine(rel, xk):
        arrived(kv.at[wrap(z + rel), c, xk], kv_recv.at[rel, c, xk])

    def go(args):
        remote(*args).start()

    mine(0, at(0))
    go(up_args(0, at(0)))
    go(dn_args(0, at(0)))
    go(dd_args(0, at(0)))

    with jax.named_scope("pool_in"):
        in_loads[3].wait()

        def pool_half(rows, value):
            pool_in[rows] = value.astype(BF)

        halves(3, pool_half)
    rim_args = (pool_in.at[pl.ds(ROWS - 16, 16)], rim, rim_send, rim_recv, nxt)
    remote(*rim_args).start()

    with jax.named_scope("own_near"):
        mine(0, at(1))
        go(up_args(0, at(1)))
        go(dd_args(0, at(1)))
        mine(0, at(3))
        go(dn_args(0, at(3)))
        go(up_args(0, at(3)))
        go(dd_args(0, at(3)))
        arrived(x_relay, x_recv)
        go(pass_args)

    with jax.named_scope("queries"):
        for s in range(2):
            arrived(qraw.at[s], q_recv.at[s])
            arrived(lamb.at[s], lam_recv.at[s])
            q = qraw[s]
            zero = jnp.zeros((64, ROWS), BF)
            qcat[s, 0] = jnp.concatenate([q[:64], zero], axis=0)
            qcat[s, 1] = jnp.concatenate([zero, q[64:]], axis=0)
            for m in range(2):
                top[s, m] = jnp.full((1, ROWS), NEG, F32)
                den[s, m] = jnp.zeros((1, ROWS), F32)
                acc[s, m] = jnp.zeros((128, ROWS), F32)

    def score(bank, zk, xk, s, m):
        keys = jnp.concatenate([kv[zk, hf, xk, 0:256] for hf in range(2)], axis=0)
        scores = jnp.dot(keys, qcat[s, m], preferred_element_type=F32)
        sbank[bank][...] = scores
        smax[bank] = jnp.max(scores, axis=0, keepdims=True)

    def weigh(bank, zk, xk, s, m, masked):
        vals = jnp.concatenate([kv[zk, hf, xk, 256 + 128 * j:384 + 128 * j] for hf in range(2) for j in range(2)],
                               axis=1)
        scores = sbank[bank][...]
        peak = smax[bank]
        if masked:
            allowed = (lax.div(lax.broadcasted_iota(jnp.int32, (ROWS, ROWS), 0), SEG)
                       <= lax.div(lax.broadcasted_iota(jnp.int32, (ROWS, ROWS), 1), SEG))
            scores = jnp.where(allowed, scores, NEG)
            peak = jnp.max(scores, axis=0, keepdims=True)
        old = top[s, m]
        new = jnp.maximum(old, peak)
        probs = jnp.exp2(scores - new)
        shrink = jnp.exp2(old - new)
        top[s, m] = new
        den[s, m] = den[s, m] * shrink + jnp.sum(probs, axis=0, keepdims=True)
        acc[s, m] = acc[s, m] * shrink + jnp.dot(vals, probs.astype(BF), preferred_element_type=F32)

    def attend(here, ahead, slots, masked):
        tiles = [(s, m) for s in slots for m in range(2)]
        for n, (s, m) in enumerate(tiles):
            if n + 1 < len(tiles):
                score((n + 1) % 2, *here, *tiles[n + 1])
            else:
                score(0, *ahead, 1, 0)
            weigh(n % 2, *here, s, m, masked == s)

    def joined(rel, xk):
        arrived(kv.at[wrap(z + rel), 1 - c, xk], kv_recv.at[rel, 1 - c, xk])

    def visit(here, ahead):
        block = here[0] * 4 + here[1]

        @pl.when(block <= qb[1])
        def _():
            @pl.when(block > qb[0])
            def _():
                @pl.when(block < qb[1])
                def _():
                    attend(here, ahead, (1,), None)

                @pl.when(block == qb[1])
                def _():
                    attend(here, ahead, (1,), 1)

            @pl.when(block <= qb[0])
            def _():
                @pl.when(block < qb[0])
                def _():
                    attend(here, ahead, (1, 0), None)

                @pl.when(block == qb[0])
                def _():
                    attend(here, ahead, (1, 0), 0)

        @pl.when(block > qb[1])
        def _():
            score(0, *ahead, 1, 0)

    below, above = (0, 1, 3, 2), (0, 3, 2, 1)
    plan = ([(0, o) for o in below] + [p for i in range(4) for p in ((3, below[i]), (1, above[i]))]
            + [(2, o) for o in (0, 3, 1, 2)])

    def near(i):
        mine(3, at(below[i]))
        if i < 2:
            go(up_args(3, at(below[i])))
        go(dd_args(3, at(below[i])))
        mine(1, at(above[i]))
        if i in (1, 2):
            go(dn_args(1, at(above[i])))
        go(dd_args(1, at(above[i])))

    def far(i):
        for off in ((0, 3), (1, 2))[i]:
            mine(2, at(off))
            go(dd_args(2, at(off)))

    def pooling(_):
        arrived(rim, rim_recv)
        edge = jnp.where(sp == 0, 0.0, rim[...].astype(F32))
        own = pool_in[...].astype(F32)
        lane = lax.broadcasted_iota(jnp.int32, (1, 128), 1)
        totals = []
        for side in range(2):
            cols = slice(128 * side, 128 * side + 128)
            line = jnp.concatenate([edge[:, cols], own[:, cols]], axis=0)
            s2 = line + pltpu.roll(line, 1, 0)
            s4 = s2 + pltpu.roll(s2, 2, 0)
            if side == 0:
                totals.append(jnp.where(lane < 64, s2, s4)[16:])
            else:
                s8 = s4 + pltpu.roll(s4, 4, 0)
                s16 = s8 + pltpu.roll(s8, 8, 0)
                totals.append(jnp.where(lane < 64, s8, s16)[16:])
        total = jnp.concatenate(totals, axis=1)
        lane = lax.broadcasted_iota(jnp.int32, (1, 256), 1)
        window = jnp.where(lane < 64, 2, jnp.where(lane < 128, 4, jnp.where(lane < 192, 8, 16)))
        position = sp * ROWS + lax.broadcasted_iota(jnp.int32, (16, 256), 0)
        early = total[:16] / jnp.minimum(position + 1, window).astype(F32)
        later = total[16:] * (1.0 / window.astype(F32))
        mixed_in = (jnp.concatenate([early, later], axis=0) - own).astype(BF)
        spread = (lax.rem(lax.broadcasted_iota(jnp.int32, (64, 256), 1), 64)
                  == lax.broadcasted_iota(jnp.int32, (64, 256), 0)).astype(F32).astype(BF)
        wide_mix = jnp.dot(pool_mix[...], spread, preferred_element_type=F32)
        same = (lax.div(lax.broadcasted_iota(jnp.int32, (256, 256), 0), 64)
                == lax.div(lax.broadcasted_iota(jnp.int32, (256, 256), 1), 64))
        block_mix = jnp.where(same, wide_mix, 0.0).astype(BF)
        grouped = jnp.dot(mixed_in, block_mix, preferred_element_type=F32)
        pooled[...] = (grouped * pool_scale[...]).astype(BF)

    def own_far(_):
        mine(0, at(2))
        go(dn_args(0, at(2)))
        go(up_args(0, at(2)))
        go(dd_args(0, at(2)))
        go(dn_args(0, at(1)))

    service = {0: (near, 0), 2: (own_far, 0), 3: (near, 1), 5: (near, 2), 7: (near, 3), 9: (pooling, 0), 10: (far, 0),
               12: (far, 1)}

    mine_h = lax.rem(x, 2)
    ret_args = [(ao.at[s], ab.at[mine_h], ret_send.at[s], ret_recv.at[mine_h], q_src[s]) for s in range(2)]

    def finish(s):
        o1 = acc[s, 0] / den[s, 0]
        o2 = acc[s, 1] / den[s, 1]
        blend = o1 - lamb[s][0:1, 0:1] * o2
        scaled = blend * lax.rsqrt(jnp.mean(blend * blend, axis=0, keepdims=True) + EPS)
        ao[s] = (scaled.T * head_gain[...] * 0.8).astype(BF)
        send_any(*ret_args[s])

    soon = wrap(z + 2) * 4 > qb[0]

    with jax.named_scope("attend"):
        joined(0, at(0))
        score(0, z, at(0), 1, 0)

        @pl.loop(0, 16)
        def _(v):
            @pl.when(pick(v, [int(i in service) for i in range(16)]) == 1)
            def _():
                for when, (serve, i) in service.items():
                    @pl.when(v == when)
                    def _():
                        with jax.named_scope(f"serve{when}"):
                            serve(i)

            @pl.when((v == 12) & soon)
            def _():
                finish(0)

            follow = jnp.minimum(v + 1, 15)
            rel, nrel = (pick(i, [p[0] for p in plan]) for i in (v, follow))
            xk, nxk = (at(pick(i, [p[1] for p in plan])) for i in (v, follow))

            @pl.when(v < 15)
            def _():
                with jax.named_scope("join"):
                    joined(nrel, nxk)

            with jax.named_scope("visit"):
                visit((wrap(z + rel), xk), (wrap(z + nrel), nxk))

    with jax.named_scope("finish"):
        finish(1)

        @pl.when(jnp.logical_not(soon))
        def _():
            finish(0)

    with jax.named_scope("drain"):
        remote(*rim_args).wait_send()
        for a in a2a_args + q_args:
            sent_any(*a)
        remote(*pass_args).wait_send()
        for off in range(4):
            remote(*up_args(0, at(off))).wait_send()
            remote(*dn_args(0, at(off))).wait_send()
            for rel in range(4):
                remote(*dd_args(rel, at(off))).wait_send()
        for i in range(2):
            remote(*up_args(3, at(below[i]))).wait_send()
            remote(*dn_args(1, at(above[i + 1]))).wait_send()

    for cp in w_loads:
        cp.wait()
    with jax.named_scope("home"):
        for hh in range(2):
            arrived(ab.at[hh], ret_recv.at[hh])

    order = [wrap(y + 2), wrap(y + 1), wrap(y - 1), y]

    def pd_args(h, k):
        return (pbuf.at[h, 2 * order[k] + 1 - c], dbuf.at[h, k], pd_send.at[h, k], pd_recv.at[h, k], partner)

    def project(h):
        feats = jnp.concatenate([pooled[...], ab[0], ab[1]], axis=1)
        term = jnp.dot(feats, w_out[:, 1024 * h:1024 * h + 1024], preferred_element_type=F32)
        pbuf[h] = term.astype(BF).reshape(8, 64, 1024)
        for k in range(4):
            go(pd_args(h, k))

    def chip_sum(h, k):
        arrived(dbuf.at[h, k], pd_recv.at[h, k])
        return pbuf[h, 2 * order[k] + c].astype(F32) + dbuf[h, k].astype(F32)

    def relay_args(h):
        return (sbuf.at[0, h], relay.at[h], y_send.at[0, h], y_recv.at[0, h], y_up if h < 2 else y_dn)

    def up_sum_args(h):
        return (sbuf.at[1, h], fin.at[0, h], y_send.at[1, h], y_recv.at[1, h], y_up)

    def dn_sum_args(h):
        return (sbuf.at[2, h], fin.at[1, h], y_send.at[2, h], y_recv.at[2, h], y_dn)

    def put(i, h, value, args):
        sbuf[i, h] = value.astype(BF)
        go(args)

    def start_relay(h):
        put(0, h, chip_sum(h, 0), relay_args(h))

    def direct(h):
        if h < 2:
            put(2, h, chip_sum(h, 2), dn_sum_args(h))
        else:
            put(1, h, chip_sum(h, 1), up_sum_args(h))

    def relayed(h):
        own_sum = chip_sum(h, 1 if h < 2 else 2)
        arrived(relay.at[h], y_recv.at[0, h])
        value = own_sum + relay[h].astype(F32)
        if h < 2:
            put(1, h, value, up_sum_args(h))
        else:
            put(2, h, value, dn_sum_args(h))

    with jax.named_scope("out_first"):
        project(0)
        project(2)
        start_relay(0)
        project(1)
        start_relay(2)
        project(3)
        start_relay(1)
        start_relay(3)
    with jax.named_scope("out_direct"):
        for h in (0, 2, 1, 3):
            direct(h)
    with jax.named_scope("out_relayed"):
        for h in (0, 2, 1, 3):
            relayed(h)
    with jax.named_scope("out_last"):
        for h in (2, 0, 3, 1):
            own_sum = chip_sum(h, 3)
            arrived(fin.at[0, h], y_recv.at[1, h])
            arrived(fin.at[1, h], y_recv.at[2, h])
            whole = own_sum + fin[0, h].astype(F32) + fin[1, h].astype(F32)
            out[:, 1024 * h:1024 * h + 1024] = whole.astype(BF)

    for a in ret_args:
        sent_any(*a)
    for h in range(4):
        for k in range(4):
            remote(*pd_args(h, k)).wait_send()
        remote(*relay_args(h)).wait_send()
        remote(*up_sum_args(h)).wait_send()
        remote(*dn_sum_args(h)).wait_send()


def body(tokens, norm_gain, w_pool_in, w_query, w_key, w_value, pool_mix, pool_scale, lam, head_gain,
         pool_proj, attn_proj):
    sd = jax.ShapeDtypeStruct
    dma = pltpu.SemaphoreType.DMA
    return pl.pallas_call(
        mixer_kernel,
        out_shape=sd((64, WIDE), BF),
        in_specs=[ANY, VM, ANY, ANY, ANY, ANY, SM, VM, VM, VM, ANY, ANY],
        out_specs=VM,
        scratch_shapes=[
            pltpu.VMEM((ROWS, WIDE), BF),
            pltpu.VMEM((ROWS, WIDE), BF),
            pltpu.VMEM((4, WIDE, 256), BF),
            pltpu.VMEM((2, 2, 512, 128), BF),
            pltpu.VMEM((2, 128, ROWS), BF),
            pltpu.VMEM((ROWS, 256), BF),
            pltpu.VMEM((2, 8, 128), F32),
            pltpu.VMEM((4, 2, 4, 512, 128), BF),
            pltpu.VMEM((2, 128, ROWS), BF),
            pltpu.VMEM((2, 2, 128, ROWS), BF),
            pltpu.VMEM((2, 8, 128), F32),
            pltpu.VMEM((16, 256), BF),
            pltpu.VMEM((2, 2, 128, ROWS), F32),
            pltpu.VMEM((2, 2, 1, ROWS), F32),
            pltpu.VMEM((2, 2, 1, ROWS), F32),
            pltpu.VMEM((ROWS, ROWS), F32),
            pltpu.VMEM((ROWS, ROWS), F32),
            pltpu.VMEM((2, 1, ROWS), F32),
            pltpu.VMEM((512, 128), BF),
            pltpu.VMEM((2, ROWS, 128), BF),
            pltpu.VMEM((2, ROWS, 128), BF),
            pltpu.VMEM((ROWS, 256), BF),
            pltpu.VMEM((512, WIDE), BF),
            pltpu.VMEM((4, 8, 64, 1024), BF),
            pltpu.VMEM((4, 4, 64, 1024), BF),
            pltpu.VMEM((3, 4, 64, 1024), BF),
            pltpu.VMEM((4, 64, 1024), BF),
            pltpu.VMEM((2, 4, 64, 1024), BF),
            dma((4,)), dma((6,)), dma, dma, dma((2, 2)), dma((4, 2, 4)), dma((2,)), dma((2,)), dma((2,)), dma((2,)),
            dma, dma, dma((2, 4)), dma((2, 4)), dma((4, 4)), dma((2,)), dma((2,)),
            dma((4, 4)), dma((4, 4)), dma((3, 4)), dma((3, 4)),
        ],
        compiler_params=pltpu.CompilerParams(vmem_limit_bytes=67043328, collective_id=0, has_side_effects=True),
        name="mixer",
    )(tokens, norm_gain.reshape(1, WIDE), w_key, w_value, w_query, w_pool_in, lam, pool_mix.reshape(256, 64),
      pool_scale.reshape(1, 256), head_gain.reshape(1, 128), pool_proj, attn_proj)


def solution(mesh):
    return jax.shard_map(
        body,
        mesh=mesh,
        in_specs=(P("sp", None), P(), P(None, "tp"), P(None, "tp"), P(None, "tp"), P(None, "tp"),
                  P("tp", None, None), P("tp"), P("tp"), P(), P("tp", None), P("tp", None)),
        out_specs=P(("sp", "tp"), None),
        check_vma=False,
    )
```

time: 77.6 us -> 73.2 us (0.943); the launches traced: 77.4 us -> 71.8 us
  Pallas kernels: 75.6 us -> 69.9 us
    pallas_call x1, Pallas kernels: 75.6 us -> 69.9 us  [body(): pl.pallas_call(mixer_kernel, out_shape=sd((64, WIDE), BF), in_specs=[ANY,...]
where the time goes in v3:
time: 73.2 us; the launch traced here: 71.8 us
  Pallas kernels  69.9 us (95%)
  local copies, waits for them, and re-layouts  1.87 us (3%)
    pallas_call x1, Pallas kernels, body(): pl.pallas_call(mixer_kernel, out_shape=sd((64, WIDE), BF), in_specs=[ANY,...  69.9 us
    unnamed x1, local copies, waits for them, and re-layouts  1.87 us

profile of v3, /device:TPU:32, one launch (start us, length us, event | category | flops | bytes accessed | tf_op | source)
XLA Modules:
  0.0 71.8 jit_solution(6671278109794067372)
XLA Ops:
  0.0 69.9 %mixer.1 = bf16[64,4096]{1,0:T(8,128)(2,1)} custom-call(bf16[512,4096]{1,0:T(8,128)(2,1)} %tok.1, f32[1,4096]{1,0:T(1,128)} %bitcast.5, bf16[4096,256]{1,0:T(8,128)(2,1)} %w_k.1, bf16[4096,256]{1,0:T(8,128)(2,1)} %w_v.1, bf16[4096,256]{1,0:T(8,128)(2,1)} %w_q.1, bf16[4096,256]{1,0:T(8,128)(2,1)} %w_p.1, f32[2]{0:T(128)} %lam.1, bf16[256,64]{1,0:T(8,128)(2,1)} %bitcast.4, ...), custom_call_target="tpu_custom_call" | custom-call | tf_op jit(solution)/shard_map/mixer/pallas_call | solution.py:545
  69.9 1.9 %copy.14 = bf16[64,4096]{1,0:T(8,128)(2,1)} copy(bf16[64,4096]{1,0:T(8,128)(2,1)} %mixer.1) | data formatting | bytes 1048576

commit v4 on v3

--- a/solution.py
+++ b/solution.py
@@ -31,13 +31,11 @@
 def inverse(table):
     return [row.index(value) for row in table for value in range(4)]
 ANY = pl.BlockSpec(memory_space=pl.ANY)
-VM = pl.BlockSpec(memory_space=pltpu.VMEM)
-SM = pl.BlockSpec(memory_space=pltpu.SMEM)
-
-
-def mixer_kernel(tok, gain, w_k, w_v, w_q, w_p, lam, pool_mix, pool_scale, head_gain, pool_proj, attn_proj,
+
+
+def mixer_kernel(tok, gain_in, w_k, w_v, w_q, w_p, lam_hbm, mix_in, scale_in, head_gain_in, pool_proj, attn_proj,
                  out,
-                 raw, normed, wts, kv_in, q_in, pool_in, lam_in, kv, qraw, qcat, lamb, rim, acc, top, den, sbank_a, sbank_b, smax, x_relay, ao, ab, pooled, w_out, pbuf, dbuf, sbuf, relay, fin,
+                 gain, lam, pool_mix, pool_scale, head_gain, out_buf, small_sem, out_sem, raw, normed, wts, kv_in, q_in, pool_in, lam_in, kv, qraw, qcat, lamb, rim, acc, top, den, sbank_a, sbank_b, smax, x_relay, ao, ab, pooled, w_out, pbuf, dbuf, sbuf, relay, fin,
                  tok_sem, w_sem, x_recv, pass_send, a2a_send, kv_recv, q_send, q_recv, lam_send, lam_recv, rim_send, rim_recv,
                  zp_send, zm_send, dd_send, ret_send, ret_recv, pd_send, pd_recv, y_send, y_recv):
     sbank = (sbank_a, sbank_b)
@@ -86,6 +84,8 @@
         return cp
 
     tok_loads = [load(tok.at[pl.ds(r * 128, 128)], raw.at[pl.ds(r * 128, 128)], tok_sem.at[r]) for r in range(4)]
+    small = [load(src, dst, small_sem.at[i]) for i, (src, dst) in enumerate(
+        ((gain_in, gain), (lam_hbm, lam), (mix_in, pool_mix), (scale_in, pool_scale), (head_gain_in, head_gain)))]
     in_loads = []
 
     barrier = pltpu.get_barrier_semaphore()
@@ -120,8 +120,7 @@
     def arrived(dst, rsem):
         pltpu.make_async_copy(dst, dst, rsem).wait()
 
-    for hh in range(2):
-        lam_in[hh] = jnp.full((8, 128), lam[hh], F32)
+    small[0].wait()
     with jax.named_scope("norm"):
         for r in range(4):
             tok_loads[r].wait()
@@ -134,14 +133,15 @@
                 scale = lax.rsqrt(jnp.mean(wide * wide, axis=-1, keepdims=True) + EPS)
                 normed[rows] = (wide * scale * gain[...]).astype(BF)
 
-    def product(i):
-        return jnp.dot(normed[...], wts[i], preferred_element_type=F32)
-
     def halves(i, finish_half):
         for r in range(2):
             rows = slice(256 * r, 256 * r + 256)
             finish_half(rows, jnp.dot(normed[rows], wts[i], preferred_element_type=F32))
 
+    for cp in small[1:]:
+        cp.wait()
+    for hh in range(2):
+        lam_in[hh] = jnp.full((8, 128), lam[hh], F32)
     with jax.named_scope("query"):
         in_loads[0].wait()
 
@@ -159,21 +159,6 @@
     for a in q_args:
         send_any(*a)
 
-    with jax.named_scope("keys_values"):
-        for i in range(1, 3):
-            in_loads[i].wait()
-        w_loads = [load(pool_proj, w_out.at[pl.ds(0, 256)], w_sem.at[4]),
-                   load(attn_proj, w_out.at[pl.ds(256, 256)], w_sem.at[5])]
-        keys = product(1).astype(BF)
-        values = product(2)
-        for hh in range(2):
-            for hf in range(2):
-                kv_in[hh, hf, 0:256] = keys[256 * hf:256 * hf + 256, 128 * hh:128 * hh + 128]
-                for j in range(2):
-                    first = 256 * hf + 128 * j
-                    tile = values[first:first + 128, 128 * hh:128 * hh + 128]
-                    kv_in[hh, hf, 256 + 128 * j:384 + 128 * j] = tile.T.astype(BF)
-
     a2a_args = []
     for hh in range(2):
         for hf in range(2):
@@ -183,21 +168,32 @@
     def hop_args(hh, hf):
         return (kv_in.at[hh, hf], x_relay, a2a_send.at[hh, hf], x_recv, dev(z, at(1 if hf == 0 else 3), hf))
 
-    for hh in range(2):
-        is_across = wrap(2 * c + hh - x) == 2
-
-        @pl.when(jnp.logical_not(is_across))
-        def _():
-            for hf in range(2):
+    def exchange(hf):
+        for hh in range(2):
+            @pl.when(wrap(2 * c + hh - x) != 2)
+            def _():
                 send_any(*a2a_args[2 * hh + hf])
 
-    for hh in range(2):
-        is_across = wrap(2 * c + hh - x) == 2
-
-        @pl.when(is_across)
-        def _():
-            for hf in range(2):
+        for hh in range(2):
+            @pl.when(wrap(2 * c + hh - x) == 2)
+            def _():
                 remote(*hop_args(hh, hf)).start()
+
+    for i in range(1, 3):
+        in_loads[i].wait()
+    for hf in range(2):
+        with jax.named_scope("keys_values"):
+            rows = slice(256 * hf, 256 * hf + 256)
+            keys = jnp.dot(normed[rows], wts[1], preferred_element_type=F32).astype(BF)
+            values = jnp.dot(normed[rows], wts[2], preferred_element_type=F32)
+            for hh in range(2):
+                kv_in[hh, hf, 0:256] = keys[:, 128 * hh:128 * hh + 128]
+                for j in range(2):
+                    tile = values[128 * j:128 * j + 128, 128 * hh:128 * hh + 128]
+                    kv_in[hh, hf, 256 + 128 * j:384 + 128 * j] = tile.T.astype(BF)
+        exchange(hf)
+    w_loads = [load(pool_proj, w_out.at[pl.ds(0, 256)], w_sem.at[4]),
+               load(attn_proj, w_out.at[pl.ds(256, 256)], w_sem.at[5])]
 
     hop_from = jnp.where(c == 0, at(3), at(1))
     pass_args = (x_relay, kv.at[z, c, hop_from], pass_send, kv_recv.at[0, c, hop_from],
@@ -509,27 +505,34 @@
         project(0)
         project(2)
         start_relay(0)
+        start_relay(2)
+        direct(0)
+        direct(2)
+    with jax.named_scope("out_second"):
         project(1)
-        start_relay(2)
         project(3)
         start_relay(1)
         start_relay(3)
-    with jax.named_scope("out_direct"):
-        for h in (0, 2, 1, 3):
-            direct(h)
+        direct(1)
+        direct(3)
     with jax.named_scope("out_relayed"):
         for h in (0, 2, 1, 3):
             relayed(h)
+    stores = []
     with jax.named_scope("out_last"):
         for h in (2, 0, 3, 1):
             own_sum = chip_sum(h, 3)
             arrived(fin.at[0, h], y_recv.at[1, h])
             arrived(fin.at[1, h], y_recv.at[2, h])
             whole = own_sum + fin[0, h].astype(F32) + fin[1, h].astype(F32)
-            out[:, 1024 * h:1024 * h + 1024] = whole.astype(BF)
+            cols = pl.ds(1024 * h, 1024)
+            out_buf[:, cols] = whole.astype(BF)
+            stores.append(load(out_buf.at[:, cols], out.at[:, cols], out_sem.at[h]))
 
     for a in ret_args:
         sent_any(*a)
+    for cp in stores:
+        cp.wait()
     for h in range(4):
         for k in range(4):
             remote(*pd_args(h, k)).wait_send()
@@ -545,9 +548,16 @@
     return pl.pallas_call(
         mixer_kernel,
         out_shape=sd((64, WIDE), BF),
-        in_specs=[ANY, VM, ANY, ANY, ANY, ANY, SM, VM, VM, VM, ANY, ANY],
-        out_specs=VM,
+        in_specs=[ANY] * 12,
+        out_specs=ANY,
         scratch_shapes=[
+            pltpu.VMEM((1, WIDE), F32),
+            pltpu.SMEM((2,), F32),
+            pltpu.VMEM((256, 64), BF),
+            pltpu.VMEM((1, 256), F32),
+            pltpu.VMEM((1, 128), F32),
+            pltpu.VMEM((64, WIDE), BF),
+            dma((5,)), dma((4,)),
             pltpu.VMEM((ROWS, WIDE), BF),
             pltpu.VMEM((ROWS, WIDE), BF),
             pltpu.VMEM((4, WIDE, 256), BF),

time: 73.2 us -> 71.8 us (0.981); the launches traced: 71.8 us -> 71.3 us
  no operation moved by 1% of the time
where the time goes in v4:
time: 71.8 us; the launch traced here: 71.3 us
  Pallas kernels  69.4 us (97%)
  local copies, waits for them, and re-layouts  1.87 us (3%)
    pallas_call x1, Pallas kernels, body(): pl.pallas_call(mixer_kernel, out_shape=sd((64, WIDE), BF), in_specs=[ANY]...  69.4 us
    unnamed x1, local copies, waits for them, and re-layouts  1.87 us

profile of v4, /device:TPU:32, one launch (start us, length us, event | category | flops | bytes accessed | tf_op | source)
XLA Modules:
  0.0 71.3 jit_solution(8535890741515632051)
XLA Ops:
  0.0 69.4 %mixer.1 = bf16[64,4096]{1,0:T(8,128)(2,1)} custom-call(bf16[512,4096]{1,0:T(8,128)(2,1)} %tok.1, f32[1,4096]{1,0:T(1,128)} %bitcast.5, bf16[4096,256]{1,0:T(8,128)(2,1)} %w_k.1, bf16[4096,256]{1,0:T(8,128)(2,1)} %w_v.1, bf16[4096,256]{1,0:T(8,128)(2,1)} %w_q.1, bf16[4096,256]{1,0:T(8,128)(2,1)} %w_p.1, f32[2]{0:T(128)} %lam_hbm.1, bf16[256,64]{1,0:T(8,128)(2,1)} %bitcast.4, ...), custom_call_target="tpu_custom_call" | custom-call | tf_op jit(solution)/shard_map/mixer/pallas_call | solution.py:548
  69.5 1.9 %copy.14 = bf16[64,4096]{1,0:T(8,128)(2,1)} copy(bf16[64,4096]{1,0:T(8,128)(2,1)} %mixer.1) | data formatting | bytes 1048576

commit v5 on v4

--- a/solution.py
+++ b/solution.py
@@ -41,17 +41,17 @@
     sbank = (sbank_a, sbank_b)
     sp = lax.axis_index("sp")
     tp = lax.axis_index("tp")
-    z, x = lax.div(sp, 4), lax.rem(sp, 4)
-    y, c = lax.div(tp, 2), lax.rem(tp, 2)
+    z, x = lax.shift_right_logical(sp, 2), sp & 3
+    y, c = lax.shift_right_logical(tp, 1), tp & 1
 
     def wrap(i):
-        return lax.rem(i + 4, 4)
+        return (i + 4) & 3
 
     def dev(zz, xx, cc):
         return (zz * 4 + xx, y * 2 + cc)
 
     def at(off):
-        return lax.rem(x + off, 4)
+        return (x + off) & 3
 
     me = (sp, tp)
 
@@ -174,6 +174,7 @@
             def _():
                 send_any(*a2a_args[2 * hh + hf])
 
+    def exchange_far(hf):
         for hh in range(2):
             @pl.when(wrap(2 * c + hh - x) == 2)
             def _():
@@ -232,6 +233,8 @@
         halves(3, pool_half)
     rim_args = (pool_in.at[pl.ds(ROWS - 16, 16)], rim, rim_send, rim_recv, nxt)
     remote(*rim_args).start()
+    for hf in range(2):
+        exchange_far(hf)
 
     with jax.named_scope("own_near"):
         mine(0, at(1))
@@ -323,8 +326,8 @@
             score(0, *ahead, 1, 0)
 
     below, above = (0, 1, 3, 2), (0, 3, 2, 1)
-    plan = ([(0, o) for o in below] + [p for i in range(4) for p in ((3, below[i]), (1, above[i]))]
-            + [(2, o) for o in (0, 3, 1, 2)])
+    plan = [(0, 0), (0, 1), (0, 3), (3, 0), (1, 0), (0, 2), (3, 1), (1, 3), (3, 3), (1, 2), (3, 2), (1, 1),
+            (2, 0), (2, 3), (2, 1), (2, 2)]
 
     def near(i):
         mine(3, at(below[i]))
@@ -381,7 +384,7 @@
         go(dd_args(0, at(2)))
         go(dn_args(0, at(1)))
 
-    service = {0: (near, 0), 2: (own_far, 0), 3: (near, 1), 5: (near, 2), 7: (near, 3), 9: (pooling, 0), 10: (far, 0),
+    service = {1: (near, 0), 3: (own_far, 0), 5: (near, 1), 7: (near, 2), 8: (near, 3), 9: (pooling, 0), 10: (far, 0),
                12: (far, 1)}
 
     mine_h = lax.rem(x, 2)

time: 71.8 us -> 71.7 us (level)
  no operation moved by 1% of the time
where the time goes in v5:
time: 71.7 us; the launch traced here: 70.8 us
  Pallas kernels  68.9 us (96%)
  local copies, waits for them, and re-layouts  1.87 us (3%)
    pallas_call x1, Pallas kernels, body(): pl.pallas_call(mixer_kernel, out_shape=sd((64, WIDE), BF), in_specs=[ANY]...  68.9 us
    unnamed x1, local copies, waits for them, and re-layouts  1.87 us

profile of v5, /device:TPU:32, one launch (start us, length us, event | category | flops | bytes accessed | tf_op | source)
XLA Modules:
  0.0 70.8 jit_solution(16103258375603245444)
XLA Ops:
  0.0 68.9 %mixer.1 = bf16[64,4096]{1,0:T(8,128)(2,1)} custom-call(bf16[512,4096]{1,0:T(8,128)(2,1)} %tok.1, f32[1,4096]{1,0:T(1,128)} %bitcast.5, bf16[4096,256]{1,0:T(8,128)(2,1)} %w_k.1, bf16[4096,256]{1,0:T(8,128)(2,1)} %w_v.1, bf16[4096,256]{1,0:T(8,128)(2,1)} %w_q.1, bf16[4096,256]{1,0:T(8,128)(2,1)} %w_p.1, f32[2]{0:T(128)} %lam_hbm.1, bf16[256,64]{1,0:T(8,128)(2,1)} %bitcast.4, ...), custom_call_target="tpu_custom_call" | custom-call | tf_op jit(solution)/shard_map/mixer/pallas_call | solution.py:551
  68.9 1.9 %copy.14 = bf16[64,4096]{1,0:T(8,128)(2,1)} copy(bf16[64,4096]{1,0:T(8,128)(2,1)} %mixer.1) | data formatting | bytes 1048576

commit v6 on v5

--- a/solution.py
+++ b/solution.py
@@ -464,8 +464,8 @@
 
     def project(h):
         feats = jnp.concatenate([pooled[...], ab[0], ab[1]], axis=1)
-        term = jnp.dot(feats, w_out[:, 1024 * h:1024 * h + 1024], preferred_element_type=F32)
-        pbuf[h] = term.astype(BF).reshape(8, 64, 1024)
+        term = jnp.dot(feats, w_out[:, 512 * h:512 * h + 512], preferred_element_type=F32)
+        pbuf[h] = term.astype(BF).reshape(8, 64, 512)
         for k in range(4):
             go(pd_args(h, k))
 
@@ -474,7 +474,7 @@
         return pbuf[h, 2 * order[k] + c].astype(F32) + dbuf[h, k].astype(F32)
 
     def relay_args(h):
-        return (sbuf.at[0, h], relay.at[h], y_send.at[0, h], y_recv.at[0, h], y_up if h < 2 else y_dn)
+        return (sbuf.at[0, h], relay.at[h], y_send.at[0, h], y_recv.at[0, h], y_up if h < 4 else y_dn)
 
     def up_sum_args(h):
         return (sbuf.at[1, h], fin.at[0, h], y_send.at[1, h], y_recv.at[1, h], y_up)
@@ -490,45 +490,40 @@
         put(0, h, chip_sum(h, 0), relay_args(h))
 
     def direct(h):
-        if h < 2:
+        if h < 4:
             put(2, h, chip_sum(h, 2), dn_sum_args(h))
         else:
             put(1, h, chip_sum(h, 1), up_sum_args(h))
 
     def relayed(h):
-        own_sum = chip_sum(h, 1 if h < 2 else 2)
+        own_sum = chip_sum(h, 1 if h < 4 else 2)
         arrived(relay.at[h], y_recv.at[0, h])
         value = own_sum + relay[h].astype(F32)
-        if h < 2:
+        if h < 4:
             put(1, h, value, up_sum_args(h))
         else:
             put(2, h, value, dn_sum_args(h))
 
     with jax.named_scope("out_first"):
-        project(0)
-        project(2)
-        start_relay(0)
-        start_relay(2)
-        direct(0)
-        direct(2)
-    with jax.named_scope("out_second"):
-        project(1)
-        project(3)
-        start_relay(1)
-        start_relay(3)
-        direct(1)
-        direct(3)
+        for h in range(4):
+            project(h)
+            project(h + 4)
+            start_relay(h)
+            start_relay(h + 4)
+            direct(h)
+            direct(h + 4)
     with jax.named_scope("out_relayed"):
-        for h in (0, 2, 1, 3):
+        for h in range(4):
             relayed(h)
+            relayed(h + 4)
     stores = []
     with jax.named_scope("out_last"):
-        for h in (2, 0, 3, 1):
+        for h in (4, 0, 5, 1, 6, 2, 7, 3):
             own_sum = chip_sum(h, 3)
             arrived(fin.at[0, h], y_recv.at[1, h])
             arrived(fin.at[1, h], y_recv.at[2, h])
             whole = own_sum + fin[0, h].astype(F32) + fin[1, h].astype(F32)
-            cols = pl.ds(1024 * h, 1024)
+            cols = pl.ds(512 * h, 512)
             out_buf[:, cols] = whole.astype(BF)
             stores.append(load(out_buf.at[:, cols], out.at[:, cols], out_sem.at[h]))
 
@@ -536,7 +531,7 @@
         sent_any(*a)
     for cp in stores:
         cp.wait()
-    for h in range(4):
+    for h in range(8):
         for k in range(4):
             remote(*pd_args(h, k)).wait_send()
         remote(*relay_args(h)).wait_send()
@@ -560,7 +555,7 @@
             pltpu.VMEM((1, 256), F32),
             pltpu.VMEM((1, 128), F32),
             pltpu.VMEM((64, WIDE), BF),
-            dma((5,)), dma((4,)),
+            dma((5,)), dma((8,)),
             pltpu.VMEM((ROWS, WIDE), BF),
             pltpu.VMEM((ROWS, WIDE), BF),
             pltpu.VMEM((4, WIDE, 256), BF),
@@ -584,14 +579,14 @@
             pltpu.VMEM((2, ROWS, 128), BF),
             pltpu.VMEM((ROWS, 256), BF),
             pltpu.VMEM((512, WIDE), BF),
-            pltpu.VMEM((4, 8, 64, 1024), BF),
-            pltpu.VMEM((4, 4, 64, 1024), BF),
-            pltpu.VMEM((3, 4, 64, 1024), BF),
-            pltpu.VMEM((4, 64, 1024), BF),
-            pltpu.VMEM((2, 4, 64, 1024), BF),
+            pltpu.VMEM((8, 8, 64, 512), BF),
+            pltpu.VMEM((8, 4, 64, 512), BF),
+            pltpu.VMEM((3, 8, 64, 512), BF),
+            pltpu.VMEM((8, 64, 512), BF),
+            pltpu.VMEM((2, 8, 64, 512), BF),
             dma((4,)), dma((6,)), dma, dma, dma((2, 2)), dma((4, 2, 4)), dma((2,)), dma((2,)), dma((2,)), dma((2,)),
             dma, dma, dma((2, 4)), dma((2, 4)), dma((4, 4)), dma((2,)), dma((2,)),
-            dma((4, 4)), dma((4, 4)), dma((3, 4)), dma((3, 4)),
+            dma((8, 4)), dma((8, 4)), dma((3, 8)), dma((3, 8)),
         ],
         compiler_params=pltpu.CompilerParams(vmem_limit_bytes=67043328, collective_id=0, has_side_effects=True),
         name="mixer",

time: 71.7 us -> 72 us (level)
  no operation moved by 1% of the time
where the time goes in v6:
time: 72 us; the launch traced here: 70.8 us
  Pallas kernels  68.9 us (96%)
  local copies, waits for them, and re-layouts  1.87 us (3%)
    pallas_call x1, Pallas kernels, body(): pl.pallas_call(mixer_kernel, out_shape=sd((64, WIDE), BF), in_specs=[ANY]...  68.9 us
    unnamed x1, local copies, waits for them, and re-layouts  1.87 us

profile of v6, /device:TPU:32, one launch (start us, length us, event | category | flops | bytes accessed | tf_op | source)
XLA Modules:
  0.0 70.8 jit_solution(3268626254496275866)
XLA Ops:
  0.0 68.9 %mixer.1 = bf16[64,4096]{1,0:T(8,128)(2,1)} custom-call(bf16[512,4096]{1,0:T(8,128)(2,1)} %tok.1, f32[1,4096]{1,0:T(1,128)} %bitcast.5, bf16[4096,256]{1,0:T(8,128)(2,1)} %w_k.1, bf16[4096,256]{1,0:T(8,128)(2,1)} %w_v.1, bf16[4096,256]{1,0:T(8,128)(2,1)} %w_q.1, bf16[4096,256]{1,0:T(8,128)(2,1)} %w_p.1, f32[2]{0:T(128)} %lam_hbm.1, bf16[256,64]{1,0:T(8,128)(2,1)} %bitcast.4, ...), custom_call_target="tpu_custom_call" | custom-call | tf_op jit(solution)/shard_map/mixer/pallas_call | solution.py:546
  68.9 1.9 %copy.14 = bf16[64,4096]{1,0:T(8,128)(2,1)} copy(bf16[64,4096]{1,0:T(8,128)(2,1)} %mixer.1) | data formatting | bytes 1048576
